TPU v7x, 32 devices: a whole 2x2x4 slice. The times are simulated.
32 devices in a mesh: sp: 8 (over z, y), tp: 4 (over x, core).
Axes of the slice: x: 2, y: 2, z: 4, core: 2. Of those that a mesh axis runs over, the one named last changes fastest.
Arguments:
- latents: bfloat16 [5120, 2048], P('sp'), may hold values from -6 to 6
- cond: float32 [2048], replicated, may hold values from -6 to 6
- ctx_cond: float32 [2048], replicated, may hold values from -6 to 6
- context: bfloat16 [768, 2048], P('sp'), may hold values from -6 to 6
- norm_gain: float32 [2048], replicated, may hold values from 0.1 to 1.9
- shift_weight: bfloat16 [2048, 2048], P('tp'), may hold values from -0.125 to 0.125
- scale_weight: bfloat16 [2048, 2048], P('tp'), may hold values from -0.125 to 0.125
- gate_weight: bfloat16 [2048, 2048], P('tp'), may hold values from -0.125 to 0.125
- q_weight: bfloat16 [2048, 1024], P(None, 'tp'), may hold values from -0.125 to 0.125
- k_weight: bfloat16 [2048, 1024], P(None, 'tp'), may hold values from -0.125 to 0.125
- v_weight: bfloat16 [2048, 1024], P(None, 'tp'), may hold values from -0.125 to 0.125
- out_weight: bfloat16 [1024, 2048], replicated, may hold values from -1.5 to 1.5
- rel_bias: float32 [8, 15, 31], P('tp'), may hold values from 1.5 to 260
Outputs:
- result: bfloat16 [5120, 2048], P(('sp', 'tp'))
All inputs are finite; a program needn't handle non-finite values.
Results may differ from a plain program's by a relative error of at most 0.0085.
Values may be sent and summed in bfloat16 or wider, within the bound.
A program may use at most 64 MiB of HBM per device.

v0:
```python
import functools

import jax
import jax.numpy as jnp
from jax import lax
from jax.experimental import pallas as pl
from jax.experimental.pallas import tpu as pltpu
from jax.sharding import PartitionSpec as P

HEAD_DIM = 128
GRID_W = 64
WIN_ROWS = 8
WIN_COLS = 16
EPS = 1e-06
NEG_BIG = -1e30
F32 = jnp.float32
BF16 = jnp.bfloat16
UP_ROWS = WIN_ROWS // 2
DOWN_ROWS = WIN_ROWS // 2 - 1
TILE = 128
PAIR = 2 * GRID_W
VMEM_BYTES = 67043328


def dot(a, b):
    return jnp.dot(a, b, preferred_element_type=F32)


def dot_t(a, b):
    return lax.dot_general(a, b, (((1,), (1,)), ((), ())), preferred_element_type=F32)


def kernel(
    ns, nt, ny,
    cond_h, ctx_cond_h, gain_h, table_h,
    lat_h, ctx_h, wsh_h, wsc_h, wg_h, wq_h, wk_h, wv_h, wo_h,
    out,
    lat, ctx, wsh, wsc, wg, wqkv, wo,
    modr, gater, mods, ctx_all, kv, q, bias, o_near, m_near, l_near, att, own, lines,
    cond, ctx_cond, gain, table,
    load_sem, mod_s, mod_r, gate_s, gate_r, ctx_s, ctx_r, halo_s, halo_r, head_s, head_r,
):
    sp, tp = lax.axis_index("sp"), lax.axis_index("tp")
    tokens, d = lat.shape
    c_here = ctx.shape[0]
    width = q.shape[1]
    heads = width // HEAD_DIM
    kt = wsh.shape[0]
    rows = tokens // GRID_W
    total_rows = rows * ns
    own_n = tokens // nt
    up_n, down_n = UP_ROWS * GRID_W, DOWN_ROWS * GRID_W
    to_log2 = 1.4426950408889634
    q_scale = HEAD_DIM ** -0.5 * to_log2

    loads = [
        pltpu.make_async_copy(s, t, load_sem.at[i])
        for i, (s, t) in enumerate([
            (wsh_h, wsh), (wsc_h, wsc), (ctx_h, ctx),
            (wk_h, wqkv.at[:, pl.ds(0, width)]), (wv_h, wqkv.at[:, pl.ds(width, width)]),
            (lat_h, lat), (wq_h, wqkv.at[:, pl.ds(2 * width, width)]), (wg_h, wg), (wo_h, wo),
            (cond_h, cond), (ctx_cond_h, ctx_cond), (gain_h, gain), (table_h, table),
        ])
    ]
    for c in loads[9:] + loads[:9]:
        c.start()

    barrier = pltpu.get_barrier_semaphore()

    def greet_tp(o, _):
        pl.semaphore_signal(barrier, inc=1, device_id={"sp": sp, "tp": (tp + o) % nt})
        return 0

    def greet_sp(o, _):
        pl.semaphore_signal(barrier, inc=1, device_id={"sp": (sp + o) % ns, "tp": tp})
        return 0

    lax.fori_loop(1, nt, greet_tp, 0)
    lax.fori_loop(1, ns, greet_sp, 0)

    for c in loads[9:]:
        c.wait()

    start = pl.multiple_of(tp * kt, 128)
    row = lax.broadcasted_iota(jnp.int32, (8, kt), 0)

    def silu(ref):
        v = ref[:, pl.ds(start, kt)]
        return jnp.broadcast_to(v / (1.0 + jnp.exp(-v)), (8, kt))

    row0_act = silu(cond)
    mixed_act = jnp.where(row % 2 == 0, row0_act, silu(ctx_cond))

    def only(a, keep):
        return jnp.where(keep, a, 0.0).astype(BF16)

    loads[0].wait()
    loads[1].wait()
    half_d = d // 2
    a_sh = [only(mixed_act, (row // 2) == 2 * k) for k in range(2)]
    a_sc = [only(mixed_act, (row // 2) == 2 * k + 1) for k in range(2)]
    step = 512
    for n0 in range(0, half_d, step):
        part = jnp.zeros((8, step), F32)
        for k in range(2):
            cols = pl.ds(k * half_d + n0, step)
            part = part + dot(a_sh[k], wsh[:, cols]) + dot(a_sc[k], wsc[:, cols])
        modr[tp, :, pl.ds(n0, step)] = part
    pl.semaphore_wait(barrier, nt - 1 + ns - 1)

    def tp_copy(buf, s_sem, r_sem, o):
        return pltpu.make_async_remote_copy(
            src_ref=buf.at[tp], dst_ref=buf.at[tp],
            send_sem=s_sem.at[o], recv_sem=r_sem.at[o],
            device_id={"sp": sp, "tp": (tp + o) % nt},
        )

    def start_mod(o, _):
        tp_copy(modr, mod_s, mod_r, o).start()
        return 0

    lax.fori_loop(1, nt, start_mod, 0)

    qc = lax.broadcasted_iota(jnp.int32, (GRID_W, PAIR), 0)
    kc = lax.broadcasted_iota(jnp.int32, (GRID_W, PAIR), 1) % GRID_W
    first = jnp.clip(qc - WIN_COLS // 2, 0, GRID_W - WIN_COLS)
    inside = (kc >= first) & (kc < first + WIN_COLS)
    lines[...] = jnp.zeros_like(lines)
    lines[:, :, 0:2 * WIN_COLS - 1] = table[...]
    for h in range(heads):
        for i in range(2 * WIN_ROWS - 2):
            near_line = jnp.broadcast_to(lines[i, h:h + 1, :], (GRID_W, PAIR))
            next_line = jnp.broadcast_to(lines[i + 1, h:h + 1, :], (GRID_W, PAIR))
            reach = WIN_COLS - 1
            rolled = pltpu.roll(near_line, PAIR - reach, 1, stride=1, stride_axis=0)
            rolled = rolled + pltpu.roll(next_line, GRID_W - reach, 1, stride=1, stride_axis=0)
            bias[h, i] = jnp.where(inside, rolled * to_log2, NEG_BIG)

    def wait_mod(o, _):
        tp_copy(modr, mod_s, mod_r, o).wait()
        return 0

    lax.fori_loop(1, nt, wait_mod, 0)
    total = modr[0]
    for i in range(1, nt):
        total = total + modr[i]
    g = gain[...]
    for k in range(2):
        cols = pl.ds(k * half_d, half_d)
        gk = g[:, k * half_d:(k + 1) * half_d]
        mods[0:1, cols] = gk * (1.0 + total[4 * k + 2:4 * k + 3])
        mods[1:2, cols] = total[4 * k:4 * k + 1]
        mods[2:3, cols] = gk * (1.0 + total[4 * k + 3:4 * k + 4])
        mods[3:4, cols] = total[4 * k + 1:4 * k + 2]

    def norm(x, r):
        xf = x.astype(F32)
        inv = lax.rsqrt(jnp.mean(xf * xf, axis=-1, keepdims=True) + EPS)
        return (xf * inv * mods[r:r + 1, :] + mods[r + 1:r + 2, :]).astype(BF16)

    loads[2].wait()
    loads[3].wait()
    loads[4].wait()
    ctx_all[sp % ny, sp // ny] = dot(norm(ctx[...], 2), wqkv[:, 0:2 * width]).astype(BF16)

    nz = ns // ny
    zi, yi = sp // ny, sp % ny

    def ctx_copy(block, dest, lane):
        return pltpu.make_async_remote_copy(
            src_ref=ctx_all.at[block % ny, block // ny],
            dst_ref=ctx_all.at[block % ny, block // ny],
            send_sem=ctx_s.at[lane, block // ny], recv_sem=ctx_r.at[block],
            device_id={"sp": dest, "tp": tp},
        )

    def across(zb, act):
        def one(o, _):
            act(ctx_copy(zb * ny + yi, zi * ny + (yi + o) % ny, 1 + o))
            return 0

        lax.fori_loop(1, ny, one, 0)

    def upward(zb, act):
        @pl.when(zi < nz - 1)
        def _():
            act(ctx_copy(zb * ny + yi, sp + ny, 0))

    def downward(zb, act):
        @pl.when(zi > 0)
        def _():
            act(ctx_copy(zb * ny + yi, sp - ny, 1))

    def go(c):
        c.start()

    def sent(c):
        c.wait_send()

    def arrived(block):
        ctx_copy(block, sp, 0).wait_recv()

    def relay(k):
        @pl.when(zi - k >= 0)
        def _():
            arrived((zi - k) * ny + yi)
            upward(zi - k, go)
            across(zi - k, go)

        @pl.when(zi + k < nz)
        def _():
            arrived((zi + k) * ny + yi)
            downward(zi + k, go)
            across(zi + k, go)

    upward(zi, go)
    downward(zi, go)
    across(zi, go)

    up = pltpu.make_async_remote_copy(
        src_ref=kv.at[pl.ds(tokens, up_n)], dst_ref=kv.at[pl.ds(0, up_n)],
        send_sem=halo_s.at[0], recv_sem=halo_r.at[0],
        device_id={"sp": (sp + 1) % ns, "tp": tp},
    )
    down = pltpu.make_async_remote_copy(
        src_ref=kv.at[pl.ds(up_n, down_n)], dst_ref=kv.at[pl.ds(up_n + tokens, down_n)],
        send_sem=halo_s.at[1], recv_sem=halo_r.at[1],
        device_id={"sp": (sp + ns - 1) % ns, "tp": tp},
    )
    has_next, has_prev = sp < ns - 1, sp > 0

    loads[5].wait()
    loads[6].wait()
    tiles = tokens // TILE
    up_tiles = pl.cdiv(up_n, TILE)
    down_tiles = pl.cdiv(down_n, TILE)

    def project(s, _):
        t = jnp.where(s < up_tiles, tiles - 1 - s, s - up_tiles)
        base = pl.multiple_of(t * TILE, TILE)
        h = norm(lat[pl.ds(base, TILE), :], 0)
        r = dot(h, wqkv[...])
        kv[pl.ds(base + up_n, TILE), :] = r[:, :2 * width].astype(BF16)
        q[pl.ds(base, TILE), :] = (r[:, 2 * width:] * q_scale).astype(BF16)

        @pl.when((s == up_tiles - 1) & has_next)
        def _():
            up.start()

        @pl.when((s == up_tiles + down_tiles - 1) & has_prev)
        def _():
            down.start()

        return 0

    lax.fori_loop(0, tiles, project, 0)

    loads[7].wait()
    seg = d // 8
    gp = jnp.zeros((8, seg), F32)
    for j in range(8):
        gp = gp + dot(only(row0_act, row == j), wg[:, pl.ds(j * seg, seg)])
    gater[tp] = gp

    def start_gate(o, _):
        tp_copy(gater, gate_s, gate_r, o).start()
        return 0

    lax.fori_loop(1, nt, start_gate, 0)

    half_t = nt // 2
    my_half = tp // half_t
    base_row = sp * rows

    def near(i, r0):
        r = r0 + i
        grid_row = base_row + r
        s_row = jnp.clip(grid_row - WIN_ROWS // 2, 0, total_rows - WIN_ROWS)
        i0 = s_row - grid_row + WIN_ROWS - 1
        win = pl.ds(pl.multiple_of((s_row - base_row + UP_ROWS) * GRID_W, GRID_W), WIN_ROWS * GRID_W)
        ids = pl.ds(pl.multiple_of(r * GRID_W, GRID_W), GRID_W)
        for h in range(heads):
            lo = h * HEAD_DIM
            b = jnp.concatenate([bias[h, i0 + 2 * k] for k in range(WIN_ROWS // 2)], axis=1)
            s = dot_t(q[ids, lo:lo + HEAD_DIM], kv[win, lo:lo + HEAD_DIM]) + b
            m = jnp.max(s, axis=-1, keepdims=True)
            e = jnp.exp2(s - m)
            l_near[h, ids, :] = jnp.sum(e, axis=-1, keepdims=True)
            m_near[h, ids, :] = m
            o_near[ids, lo:lo + HEAD_DIM] = dot(
                e.astype(BF16), kv[win, width + lo:width + lo + HEAD_DIM]
            )
        return r0

    relay(1)
    mid = rows - UP_ROWS - DOWN_ROWS
    lax.fori_loop(0, mid, near, UP_ROWS, unroll=True)
    if nz > 2:
        relay(2)

    @pl.when(has_next)
    def _():
        down.wait_recv()
        up.wait_send()

    @pl.when(has_prev)
    def _():
        up.wait_recv()
        down.wait_send()

    lax.fori_loop(0, DOWN_ROWS, near, rows - DOWN_ROWS, unroll=True)
    if nz > 3:
        relay(3)
    lax.fori_loop(0, UP_ROWS, near, 0, unroll=True)

    def late_relay(k, _):
        relay(k)
        return 0

    lax.fori_loop(4, nz, late_relay, 0)

    def flat(x):
        if c_here % 16:
            return x.astype(F32).reshape(nz * c_here, HEAD_DIM).astype(BF16)
        return x.reshape(nz * c_here, HEAD_DIM)

    far_tile = tokens // 4

    def far(t, o, last):
        ids = pl.ds(pl.multiple_of(t * far_tile, 16), far_tile)
        col = (yi + o) % ny
        for h in range(heads):
            lo = h * HEAD_DIM
            ck = flat(ctx_all[col, :, :, lo:lo + HEAD_DIM])
            cv = flat(ctx_all[col, :, :, width + lo:width + lo + HEAD_DIM])
            s = dot_t(q[ids, lo:lo + HEAD_DIM], ck)
            mn = m_near[h, ids, :]
            m = jnp.maximum(jnp.max(s, axis=-1, keepdims=True), mn)
            e = jnp.exp2(s - m)
            w = jnp.exp2(mn - m)
            l = jnp.sum(e, axis=-1, keepdims=True) + w * l_near[h, ids, :]
            acc = dot(e.astype(BF16), cv) + w * o_near[ids, lo:lo + HEAD_DIM]
            if last:
                att[ids, lo:lo + HEAD_DIM] = (acc / l).astype(BF16)
            else:
                m_near[h, ids, :] = m
                l_near[h, ids, :] = l
                o_near[ids, lo:lo + HEAD_DIM] = acc

    def far_all(o, _):
        for t in range(4):
            far(t, o, False)
        return 0

    if ny > 1:
        far_all(0, 0)

    def settle_row(zb, _):
        def other(o, _):
            arrived(zb * ny + (yi + o) % ny)
            return 0

        lax.fori_loop(1, ny, other, 0)
        across(zb, sent)

        @pl.when(zb <= zi)
        def _():
            upward(zb, sent)

        @pl.when(zb >= zi)
        def _():
            downward(zb, sent)

        return 0

    lax.fori_loop(0, nz, settle_row, 0)

    lax.fori_loop(1, ny - 1, far_all, 0)

    def head_copy(src, dst):
        return pltpu.make_async_remote_copy(
            src_ref=att.at[pl.ds(pl.multiple_of(dst * own_n, 16), own_n)], dst_ref=own.at[src],
            send_sem=head_s.at[dst], recv_sem=head_r.at[src],
            device_id={"sp": sp, "tp": dst},
        )

    far((1 - my_half) * 2, ny - 1, True)
    far((1 - my_half) * 2 + 1, ny - 1, True)

    def send_other(j, _):
        head_copy(tp, (1 - my_half) * half_t + j).start()
        return 0

    lax.fori_loop(0, half_t, send_other, 0)
    far(my_half * 2, ny - 1, True)
    far(my_half * 2 + 1, ny - 1, True)

    def mate(o):
        return my_half * half_t + (tp + o) % half_t

    def send_same(o, _):
        head_copy(tp, mate(o)).start()
        return 0

    lax.fori_loop(1, half_t, send_same, 0)

    def wait_gate(o, _):
        tp_copy(gater, gate_s, gate_r, o).wait()
        return 0

    lax.fori_loop(1, nt, wait_gate, 0)
    gsum = gater[0]
    for i in range(1, nt):
        gsum = gsum + gater[i]
    gates = jnp.concatenate([gsum[j:j + 1] for j in range(8)], axis=1)
    loads[8].wait()
    own[tp] = att[pl.ds(pl.multiple_of(tp * own_n, 16), own_n), :]

    def settle(o, _):
        p = (tp + o) % nt
        head_copy(tp, p).wait_send()
        head_copy(p, p).wait_recv()
        return 0

    lax.fori_loop(1, nt, settle, 0)
    a = jnp.concatenate([own[i] for i in range(nt)], axis=1)
    my_rows = pl.ds(pl.multiple_of(tp * own_n, 16), own_n)
    for n0 in range(0, d, 512):
        y = dot(a, wo[:, n0:n0 + 512])
        out[:, n0:n0 + 512] = (
            lat[my_rows, n0:n0 + 512].astype(F32) + gates[:, n0:n0 + 512] * y
        ).astype(BF16)


def shards(
    ns, nt,
    latents, cond, ctx_cond, context, norm_gain, shift_weight, scale_weight, gate_weight,
    q_weight, k_weight, v_weight, out_weight, rel_bias,
):
    tokens, d = latents.shape
    c_here = context.shape[0]
    kt = shift_weight.shape[0]
    width = q_weight.shape[1]
    heads = width // HEAD_DIM
    own_n = tokens // nt
    table = jnp.transpose(rel_bias, (1, 0, 2))
    ny = 1
    while ns % (2 * ny) == 0 and 4 * ny * ny <= ns:
        ny *= 2
    halo = (UP_ROWS + DOWN_ROWS) * GRID_W
    vmem = pl.BlockSpec(memory_space=pltpu.VMEM)
    hbm = pl.BlockSpec(memory_space=pltpu.HBM)
    sem = pltpu.SemaphoreType.DMA
    return pl.pallas_call(
        functools.partial(kernel, ns, nt, ny),
        out_shape=jax.ShapeDtypeStruct((own_n, d), BF16),
        in_specs=[hbm] * 13,
        out_specs=vmem,
        scratch_shapes=[
            pltpu.VMEM((tokens, d), BF16),
            pltpu.VMEM((c_here, d), BF16),
            pltpu.VMEM((kt, d), BF16),
            pltpu.VMEM((kt, d), BF16),
            pltpu.VMEM((kt, d), BF16),
            pltpu.VMEM((d, 3 * width), BF16),
            pltpu.VMEM(out_weight.shape, BF16),
            pltpu.VMEM((nt, 8, d // 2), F32),
            pltpu.VMEM((nt, 8, d // 8), F32),
            pltpu.VMEM((8, d), F32),
            pltpu.VMEM((ny, ns // ny, c_here, 2 * width), BF16),
            pltpu.VMEM((tokens + halo, 2 * width), BF16),
            pltpu.VMEM((tokens, width), BF16),
            pltpu.VMEM((heads, 2 * WIN_ROWS - 2, GRID_W, PAIR), F32),
            pltpu.VMEM((tokens, width), F32),
            pltpu.VMEM((heads, tokens, 1), F32),
            pltpu.VMEM((heads, tokens, 1), F32),
            pltpu.VMEM((tokens, width), BF16),
            pltpu.VMEM((nt, own_n, width), BF16),
            pltpu.VMEM((2 * WIN_ROWS - 1, heads, PAIR), F32),
            pltpu.VMEM((1, d), F32),
            pltpu.VMEM((1, d), F32),
            pltpu.VMEM((1, d), F32),
            pltpu.VMEM(table.shape, F32),
            sem((13,)),
            sem((nt,)), sem((nt,)), sem((nt,)), sem((nt,)),
            sem((ny + 1, ns // ny)), sem((ns,)),
            sem((2,)), sem((2,)),
            sem((nt,)), sem((nt,)),
        ],
        compiler_params=pltpu.CompilerParams(
            collective_id=0, has_side_effects=True, vmem_limit_bytes=VMEM_BYTES - own_n * d * 2 - 300 * 1024
        ),
    )(
        cond[None], ctx_cond[None], norm_gain[None], table, latents, context, shift_weight, scale_weight, gate_weight,
        q_weight, k_weight, v_weight, out_weight,
    )


def solution(mesh):
    in_specs = (
        P("sp", None),
        P(),
        P(),
        P("sp", None),
        P(),
        P("tp", None),
        P("tp", None),
        P("tp", None),
        P(None, "tp"),
        P(None, "tp"),
        P(None, "tp"),
        P(),
        P("tp", None, None),
    )
    body = functools.partial(shards, mesh.shape["sp"], mesh.shape["tp"])
    return jax.shard_map(
        body, mesh=mesh, in_specs=in_specs, out_specs=P(("sp", "tp"), None), check_vma=False
    )
```

profile of v0, /device:TPU:1, one launch (start us, length us, event | category | flops | bytes accessed | tf_op | source)
XLA Modules:
  0.0 38.8 jit_solution(1964552550634267493)
XLA Ops:
  0.0 36.8 %shard_map.127 = bf16[160,2048]{1,0:T(8,128)(2,1)} custom-call(f32[1,2048]{1,0:T(1,128)} %bitcast.5, f32[1,2048]{1,0:T(1,128)} %bitcast.6, f32[1,2048]{1,0:T(1,128)} %bitcast.7, f32[15,2,31]{2,1,0:T(2,128)} %bitcast.4, bf16[640,2048]{1,0:T(8,128)(2,1)} %lat_h.1, bf16[96,2048]{1,0:T(8,128)(2,1)} %ctx_h.1, bf16[512,2048]{1,0:T(8,128)(2,1)} %wsh_h.1, ...), custom_call_target="tpu_custom_call" | custom-call | tf_op jit(solution)/shard_map/pallas_call | solution.py:454
  36.8 2.0 %copy.15 = bf16[160,2048]{1,0:T(8,128)(2,1)} copy(bf16[160,2048]{1,0:T(8,128)(2,1)} %shard_map.127) | data formatting | bytes 1310720
where the time goes:
time: 39.1 us; the launch traced here: 38.8 us
  Pallas kernels  36.8 us (94%)
  local copies, waits for them, and re-layouts  1.98 us (5%)
    pallas_call x1, Pallas kernels, shards(): pl.pallas_call(functools.partial(kernel, ns, nt, ny), out_shape=jax.Shape...  36.8 us
    unnamed x1, local copies, waits for them, and re-layouts  1.98 us

commit v1 on v0

v1 whole, which is shorter than its diff:
```python
import functools

import jax
import jax.numpy as jnp
from jax import lax
from jax.experimental import pallas as pl
from jax.experimental.pallas import tpu as pltpu
from jax.sharding import PartitionSpec as P

HEAD_DIM = 128
GRID_W = 64
WIN_ROWS = 8
WIN_COLS = 16
EPS = 1e-06
NEG_BIG = -1e30
F32 = jnp.float32
BF16 = jnp.bfloat16
UP_ROWS = WIN_ROWS // 2
DOWN_ROWS = WIN_ROWS // 2 - 1
PAIR = 2 * GRID_W
KEY_ROWS = WIN_ROWS + 2
KEYS = KEY_ROWS * GRID_W
TABLES = 2 * WIN_ROWS - 2
VMEM_BYTES = 67043328


def dot(a, b):
    return jnp.dot(a, b, preferred_element_type=F32)


def dot_t(a, b):
    return lax.dot_general(a, b, (((1,), (1,)), ((), ())), preferred_element_type=F32)


def wide(x, n):
    if n % HEAD_DIM:
        return x[:, 0:1]
    return jnp.concatenate([x] * (n // HEAD_DIM), axis=1)


def kernel(
    ns, nt, ny,
    cond_h, ctx_cond_h, gain_h, table_h,
    lat_h, ctx_h, wsh_h, wsc_h, wg_h, wq_h, wk_h, wv_h, wo_h,
    own, wo, gates, lat_own,
    lat, ctx, wsh, wsc, wg, wqkv,
    modr, gater, mods, inv, hbuf, ctx_all, kv, q, bias, s_near, s_far, acc, mx, att, lines,
    cond, ctx_cond, gain, table,
    load_sem, mod_s, mod_r, gate_s, gate_r, ctx_s, ctx_r, halo_s, halo_r, head_s, head_r,
):
    sp, tp = lax.axis_index("sp"), lax.axis_index("tp")
    tokens, d = lat.shape
    c_here = ctx.shape[0]
    width = q.shape[1]
    heads = width // HEAD_DIM
    kt = wsh.shape[0]
    rows = tokens // GRID_W
    total_rows = rows * ns
    own_n = tokens // nt
    up_n, down_n = UP_ROWS * GRID_W, DOWN_ROWS * GRID_W
    to_log2 = 1.4426950408889634
    q_scale = HEAD_DIM ** -0.5 * to_log2
    half_d = d // 2
    step = 512

    count = [0]

    def load(s, t):
        c = pltpu.make_async_copy(s, t, load_sem.at[count[0]])
        count[0] += 1
        return c

    small = [load(cond_h, cond), load(ctx_cond_h, ctx_cond), load(gain_h, gain), load(table_h, table)]
    mod_loads = []
    for n0 in range(0, half_d, step):
        mod_loads.append([
            load(s.at[:, pl.ds(k * half_d + n0, step)], t.at[:, pl.ds(k * half_d + n0, step)])
            for k in range(2) for s, t in ((wsh_h, wsh), (wsc_h, wsc))
        ])
    ctx_load, lat_load, wg_load = load(ctx_h, ctx), load(lat_h, lat), load(wg_h, wg)
    wk_load = load(wk_h, wqkv.at[:, pl.ds(0, width)])
    wv_load = load(wv_h, wqkv.at[:, pl.ds(width, width)])
    wq_load = load(wq_h, wqkv.at[:, pl.ds(2 * width, width)])
    wo_load = load(wo_h, wo)
    my_rows = pl.ds(pl.multiple_of(tp * own_n, 16), own_n)
    own_load = load(lat_h.at[my_rows], lat_own)
    for c in small + sum(mod_loads, []) + [ctx_load, lat_load, wg_load, wk_load, wv_load, wq_load, wo_load, own_load]:
        c.start()

    barrier = pltpu.get_barrier_semaphore()

    def greet_tp(o, _):
        pl.semaphore_signal(barrier, inc=1, device_id={"sp": sp, "tp": (tp + o) % nt})
        return 0

    def greet_sp(o, _):
        pl.semaphore_signal(barrier, inc=1, device_id={"sp": (sp + o) % ns, "tp": tp})
        return 0

    lax.fori_loop(1, nt, greet_tp, 0)
    lax.fori_loop(1, ns, greet_sp, 0)

    for c in small:
        c.wait()

    start = pl.multiple_of(tp * kt, 128)
    row = lax.broadcasted_iota(jnp.int32, (8, kt), 0)

    def silu(ref):
        v = ref[:, pl.ds(start, kt)]
        return jnp.broadcast_to(v / (1.0 + jnp.exp(-v)), (8, kt))

    row0_act = silu(cond)
    mixed_act = jnp.where(row % 2 == 0, row0_act, silu(ctx_cond))

    def only(a, keep):
        return jnp.where(keep, a, 0.0).astype(BF16)

    a_sh = [only(mixed_act, (row // 2) == 2 * k) for k in range(2)]
    a_sc = [only(mixed_act, (row // 2) == 2 * k + 1) for k in range(2)]
    for i, n0 in enumerate(range(0, half_d, step)):
        part = jnp.zeros((8, step), F32)
        for k in range(2):
            cols = pl.ds(k * half_d + n0, step)
            mod_loads[i][2 * k].wait()
            part = part + dot(a_sh[k], wsh[:, cols])
            mod_loads[i][2 * k + 1].wait()
            part = part + dot(a_sc[k], wsc[:, cols])
        modr[tp, :, pl.ds(n0, step)] = part
    pl.semaphore_wait(barrier, nt - 1 + ns - 1)

    def tp_copy(buf, s_sem, r_sem, o):
        return pltpu.make_async_remote_copy(
            src_ref=buf.at[tp], dst_ref=buf.at[tp],
            send_sem=s_sem.at[o], recv_sem=r_sem.at[o],
            device_id={"sp": sp, "tp": (tp + o) % nt},
        )

    def start_mod(o, _):
        tp_copy(modr, mod_s, mod_r, o).start()
        return 0

    lax.fori_loop(1, nt, start_mod, 0)

    qc = lax.broadcasted_iota(jnp.int32, (GRID_W, PAIR), 0)
    lane = lax.broadcasted_iota(jnp.int32, (GRID_W, PAIR), 1)
    kc = lane % GRID_W
    first = jnp.clip(qc - WIN_COLS // 2, 0, GRID_W - WIN_COLS)
    inside = (kc >= first) & (kc < first + WIN_COLS)
    lines[...] = jnp.zeros_like(lines)
    lines[:, :, 0:2 * WIN_COLS - 1] = table[...]
    low_row = WIN_ROWS - 1 - WIN_ROWS // 2
    for h in range(heads):
        for i in range(TABLES):
            near_line = jnp.broadcast_to(lines[i, h:h + 1, :], (GRID_W, PAIR))
            next_line = jnp.broadcast_to(lines[i + 1, h:h + 1, :], (GRID_W, PAIR))
            reach = WIN_COLS - 1
            rolled = pltpu.roll(near_line, PAIR - reach, 1, stride=1, stride_axis=0)
            rolled = rolled + pltpu.roll(next_line, GRID_W - reach, 1, stride=1, stride_axis=0)
            both = jnp.where(inside, rolled * to_log2, NEG_BIG)
            bias[h, i] = both
            if i == low_row - 1:
                bias[h, TABLES] = jnp.where(lane >= GRID_W, both, NEG_BIG)
            if i == low_row + WIN_ROWS - 1:
                bias[h, TABLES + 1] = jnp.where(lane < GRID_W, both, NEG_BIG)
        bias[h, TABLES + 2] = jnp.full((GRID_W, PAIR), NEG_BIG, F32)
    mx[...] = jnp.full_like(mx, NEG_BIG)
    acc[...] = jnp.zeros_like(acc)
    n_keys = kv.shape[0] - tokens - up_n

    @pl.when(sp == 0)
    def _():
        kv[0:up_n, :] = jnp.zeros((up_n, 2 * width), BF16)

    @pl.when(sp == ns - 1)
    def _():
        kv[pl.ds(up_n + tokens, down_n), :] = jnp.zeros((down_n, 2 * width), BF16)

    kv[pl.ds(up_n + tokens + down_n, n_keys - down_n), :] = jnp.zeros((n_keys - down_n, 2 * width), BF16)

    def inv_of(x):
        xf = x.astype(F32)
        return lax.rsqrt(jnp.mean(xf * xf, axis=-1, keepdims=True) + EPS)

    ctx_load.wait()
    ctx_inv = inv_of(ctx[...])
    lat_load.wait()
    for t in range(0, tokens, GRID_W):
        inv[t:t + GRID_W, :] = jnp.broadcast_to(inv_of(lat[t:t + GRID_W, :]), (GRID_W, HEAD_DIM))

    wg_load.wait()
    seg = d // 8
    gp = jnp.zeros((8, seg), F32)
    for j in range(8):
        gp = gp + dot(only(row0_act, row == j), wg[:, pl.ds(j * seg, seg)])
    gater[tp] = gp

    def start_gate(o, _):
        tp_copy(gater, gate_s, gate_r, o).start()
        return 0

    lax.fori_loop(1, nt, start_gate, 0)
    wk_load.wait()
    wv_load.wait()

    def wait_mod(o, _):
        tp_copy(modr, mod_s, mod_r, o).wait()
        return 0

    lax.fori_loop(1, nt, wait_mod, 0)
    total = modr[0]
    for i in range(1, nt):
        total = total + modr[i]
    g = gain[...]
    for k in range(2):
        cols = pl.ds(k * half_d, half_d)
        gk = g[:, k * half_d:(k + 1) * half_d]
        mods[0:1, cols] = gk * (1.0 + total[4 * k + 2:4 * k + 3])
        mods[1:2, cols] = total[4 * k:4 * k + 1]
        mods[2:3, cols] = gk * (1.0 + total[4 * k + 3:4 * k + 4])
        mods[3:4, cols] = total[4 * k + 1:4 * k + 2]

    ctx_hid = (ctx[...].astype(F32) * ctx_inv * mods[2:3, :] + mods[3:4, :]).astype(BF16)
    ctx_all[sp % ny, sp // ny] = dot(ctx_hid, wqkv[:, 0:2 * width]).astype(BF16)

    nz = ns // ny
    zi, yi = sp // ny, sp % ny

    def ctx_copy(block, dest, lane):
        return pltpu.make_async_remote_copy(
            src_ref=ctx_all.at[block % ny, block // ny],
            dst_ref=ctx_all.at[block % ny, block // ny],
            send_sem=ctx_s.at[lane, block // ny], recv_sem=ctx_r.at[block],
            device_id={"sp": dest, "tp": tp},
        )

    def across(zb, act):
        def one(o, _):
            act(ctx_copy(zb * ny + yi, zi * ny + (yi + o) % ny, 1 + o))
            return 0

        lax.fori_loop(1, ny, one, 0)

    def upward(zb, act):
        @pl.when(zi < nz - 1)
        def _():
            act(ctx_copy(zb * ny + yi, sp + ny, 0))

    def downward(zb, act):
        @pl.when(zi > 0)
        def _():
            act(ctx_copy(zb * ny + yi, sp - ny, 1))

    def go(c):
        c.start()

    def sent(c):
        c.wait_send()

    def arrived(block):
        ctx_copy(block, sp, 0).wait_recv()

    def relay(k):
        @pl.when(zi - k >= 0)
        def _():
            arrived((zi - k) * ny + yi)
            upward(zi - k, go)
            across(zi - k, go)

        @pl.when(zi + k < nz)
        def _():
            arrived((zi + k) * ny + yi)
            downward(zi + k, go)
            across(zi + k, go)

    upward(zi, go)
    downward(zi, go)
    across(zi, go)

    up = pltpu.make_async_remote_copy(
        src_ref=kv.at[pl.ds(tokens, up_n)], dst_ref=kv.at[pl.ds(0, up_n)],
        send_sem=halo_s.at[0], recv_sem=halo_r.at[0],
        device_id={"sp": (sp + 1) % ns, "tp": tp},
    )
    down = pltpu.make_async_remote_copy(
        src_ref=kv.at[pl.ds(up_n, down_n)], dst_ref=kv.at[pl.ds(up_n + tokens, down_n)],
        send_sem=halo_s.at[1], recv_sem=halo_r.at[1],
        device_id={"sp": (sp + ns - 1) % ns, "tp": tp},
    )
    has_next, has_prev = sp < ns - 1, sp > 0

    wq_load.wait()
    spans = [(tokens - up_n, up_n), (0, down_n), (down_n, tokens - up_n - down_n)]

    def hidden(i):
        lo, n = spans[i]
        x = lat[lo:lo + n, :].astype(F32)
        h = x * wide(inv[lo:lo + n, :], d) * mods[0:1, :] + mods[1:2, :]
        hbuf[i % 2, 0:n, :] = h.astype(BF16)

    hidden(0)
    for i, (lo, n) in enumerate(spans):
        r = dot(hbuf[i % 2, 0:n, :], wqkv[...])
        kv[lo + up_n:lo + up_n + n, :] = r[:, :2 * width].astype(BF16)
        q[lo:lo + n, :] = (r[:, 2 * width:] * q_scale).astype(BF16)
        if i + 1 < len(spans):
            hidden(i + 1)
        if i == 0:
            pl.when(has_next)(lambda: up.start())
        if i == 1:
            pl.when(has_prev)(lambda: down.start())

    half_t = nt // 2
    my_half = tp // half_t
    base_row = sp * rows
    ones = jnp.ones((1, HEAD_DIM), BF16)

    def with_ones(v):
        return jnp.concatenate([v, jnp.broadcast_to(ones, v.shape)], axis=1)

    def window(r):
        grid_row = base_row + r
        s0 = jnp.clip(grid_row - WIN_ROWS // 2, 0, total_rows - WIN_ROWS)
        s1 = jnp.clip(grid_row + 1 - WIN_ROWS // 2, 0, total_rows - WIN_ROWS)
        win = pl.ds(pl.multiple_of((s0 - base_row + UP_ROWS) * GRID_W, GRID_W), KEYS)
        return grid_row, s0, s1, win

    def near_scores(r, h):
        grid_row, s0, s1, win = window(r)
        i0 = s0 - grid_row + WIN_ROWS - 1
        i1 = i0 - 1
        moved = s1 > s0
        lo = h * HEAD_DIM
        t = r * GRID_W
        s = dot_t(q[t:t + PAIR, lo:lo + HEAD_DIM], kv[win, lo:lo + HEAD_DIM])
        b0 = [bias[h, i0 + 2 * k] for k in range(WIN_ROWS // 2)]
        ids = [jnp.where(moved, TABLES, i1)]
        ids += [jnp.where(moved, i1 + 2 * k, i1 + 2 * k) for k in range(1, WIN_ROWS // 2)]
        ids += [jnp.where(moved, TABLES + 1, TABLES + 2)]
        b1 = [bias[h, i] for i in ids]
        x0 = s[:GRID_W, :WIN_ROWS * GRID_W] + jnp.concatenate(b0, axis=1)
        x1 = s[GRID_W:, :] + jnp.concatenate(b1, axis=1)
        s_near[h, t:t + GRID_W, 0:WIN_ROWS * GRID_W] = x0
        s_near[h, t + GRID_W:t + PAIR, :] = x1
        m = jnp.concatenate([jnp.max(x0, axis=-1, keepdims=True), jnp.max(x1, axis=-1, keepdims=True)], axis=0)
        return jnp.broadcast_to(m, (PAIR, HEAD_DIM))

    def near_values(r, h, m):
        win = window(r)[3]
        lo = h * HEAD_DIM
        t = r * GRID_W
        old = mx[h, t:t + PAIR, :]
        m = jnp.maximum(m, old)
        w = jnp.exp2(old - m)
        n0 = WIN_ROWS * GRID_W
        e0 = jnp.exp2(s_near[h, t:t + GRID_W, 0:n0] - wide(m[:GRID_W], n0)).astype(BF16)
        e1 = jnp.exp2(s_near[h, t + GRID_W:t + PAIR, :] - wide(m[GRID_W:], KEYS)).astype(BF16)
        e0 = jnp.concatenate([e0, jnp.zeros((GRID_W, KEYS - n0), BF16)], axis=1)
        p = jnp.concatenate([e0, e1], axis=0)
        o = dot(p, with_ones(kv[win, width + lo:width + lo + HEAD_DIM]))
        mx[h, t:t + PAIR, :] = m
        acc[h, t:t + PAIR, :] = acc[h, t:t + PAIR, :] * wide(w, 2 * HEAD_DIM) + o

    def near(pairs):
        units = [(r, h) for r in pairs for h in range(heads)]
        ms = [near_scores(r, h) for r, h in units]
        for (r, h), m in zip(units, ms):
            near_values(r, h, m)

    def flat(x):
        if c_here % 16:
            return x.astype(F32).reshape(nz * c_here, HEAD_DIM).astype(BF16)
        return x.reshape(nz * c_here, HEAD_DIM)

    far_n = nz * c_here

    def far_scores(t, col, h):
        lo = h * HEAD_DIM
        s = dot_t(q[t, lo:lo + HEAD_DIM], flat(ctx_all[col, :, :, lo:lo + HEAD_DIM]))
        s_far[h, t, :] = s
        return jnp.broadcast_to(jnp.max(s, axis=-1, keepdims=True), (own_n, HEAD_DIM))

    def far_values(t, col, h, m, last):
        lo = h * HEAD_DIM
        old = mx[h, t, :]
        m = jnp.maximum(m, old)
        w = jnp.exp2(old - m)
        e = jnp.exp2(s_far[h, t, :] - wide(m, far_n)).astype(BF16)
        o = dot(e, with_ones(flat(ctx_all[col, :, :, width + lo:width + lo + HEAD_DIM])))
        o = acc[h, t, :] * wide(w, 2 * HEAD_DIM) + o
        if last:
            att[t, lo:lo + HEAD_DIM] = (o[:, :HEAD_DIM] / o[:, HEAD_DIM:]).astype(BF16)
        else:
            mx[h, t, :] = m
            acc[h, t, :] = o

    def far(parts, o, last):
        col = (yi + o) % ny
        units = [(pl.ds(pl.multiple_of(p * own_n, 16), own_n), h) for p in parts for h in range(heads)]
        ms = [far_scores(t, col, h) for t, h in units]
        for (t, h), m in zip(units, ms):
            far_values(t, col, h, m, last)

    def far_all(o, _):
        far(range(nt), o, False)
        return 0

    near(range(UP_ROWS, rows - UP_ROWS, 2))
    relay(1)
    if nz > 2:
        relay(2)
    if nz > 3:
        relay(3)

    def late_relay(k, _):
        relay(k)
        return 0

    lax.fori_loop(4, nz, late_relay, 0)
    if ny > 1:
        far_all(0, 0)

    @pl.when(has_next)
    def _():
        down.wait_recv()
        up.wait_send()

    @pl.when(has_prev)
    def _():
        up.wait_recv()
        down.wait_send()

    near([*range(0, UP_ROWS, 2), *range(rows - UP_ROWS, rows, 2)])

    def settle_row(zb, _):
        def other(o, _):
            arrived(zb * ny + (yi + o) % ny)
            return 0

        lax.fori_loop(1, ny, other, 0)
        across(zb, sent)

        @pl.when(zb <= zi)
        def _():
            upward(zb, sent)

        @pl.when(zb >= zi)
        def _():
            downward(zb, sent)

        return 0

    lax.fori_loop(0, nz, settle_row, 0)

    lax.fori_loop(1, ny - 1, far_all, 0)

    def head_copy(src, dst):
        return pltpu.make_async_remote_copy(
            src_ref=att.at[pl.ds(pl.multiple_of(dst * own_n, 16), own_n)], dst_ref=own.at[src],
            send_sem=head_s.at[dst], recv_sem=head_r.at[src],
            device_id={"sp": sp, "tp": dst},
        )

    other_half = (1 - my_half) * half_t
    far([other_half + j for j in range(half_t)], ny - 1, True)

    def send_other(j, _):
        head_copy(tp, (1 - my_half) * half_t + j).start()
        return 0

    lax.fori_loop(0, half_t, send_other, 0)
    far([my_half * half_t + j for j in range(half_t)], ny - 1, True)

    def mate(o):
        return my_half * half_t + (tp + o) % half_t

    def send_same(o, _):
        head_copy(tp, mate(o)).start()
        return 0

    lax.fori_loop(1, half_t, send_same, 0)

    def wait_gate(o, _):
        tp_copy(gater, gate_s, gate_r, o).wait()
        return 0

    lax.fori_loop(1, nt, wait_gate, 0)
    gsum = gater[0]
    for i in range(1, nt):
        gsum = gsum + gater[i]
    gates[...] = jnp.concatenate([gsum[j:j + 1] for j in range(8)], axis=1)
    own[tp] = att[my_rows, :]
    wo_load.wait()
    own_load.wait()

    def settle(o, _):
        p = (tp + o) % nt
        head_copy(tp, p).wait_send()
        head_copy(p, p).wait_recv()
        return 0

    lax.fori_loop(1, nt, settle, 0)


def finish(own, wo, gates, lat_own, out, buf, sem):
    nt = own.shape[0]
    d = wo.shape[1]
    step = d // 4
    a = jnp.concatenate([own[i] for i in range(nt)], axis=1)
    copies = []
    for i in range(4):
        cols = pl.ds(i * step, step)
        y = dot(a, wo[:, cols])
        buf[:, cols] = (lat_own[:, cols].astype(F32) + gates[:, cols] * y).astype(BF16)
        copies.append(pltpu.make_async_copy(buf.at[:, cols], out.at[:, cols], sem.at[i]))
        copies[-1].start()
    for c in copies:
        c.wait()


def shards(
    ns, nt,
    latents, cond, ctx_cond, context, norm_gain, shift_weight, scale_weight, gate_weight,
    q_weight, k_weight, v_weight, out_weight, rel_bias,
):
    tokens, d = latents.shape
    c_here = context.shape[0]
    kt = shift_weight.shape[0]
    width = q_weight.shape[1]
    heads = width // HEAD_DIM
    own_n = tokens // nt
    table = jnp.transpose(rel_bias, (1, 0, 2))
    ny = 1
    while ns % (2 * ny) == 0 and 4 * ny * ny <= ns:
        ny *= 2
    halo = (UP_ROWS + DOWN_ROWS + 1) * GRID_W
    vmem = pl.BlockSpec(memory_space=pltpu.VMEM)
    hbm = pl.BlockSpec(memory_space=pltpu.HBM)
    sem = pltpu.SemaphoreType.DMA
    tail = 8 * 1024 * 1024
    parts = pl.pallas_call(
        functools.partial(kernel, ns, nt, ny),
        out_shape=(
            pltpu.VMEM((nt, own_n, width), BF16),
            pltpu.VMEM(out_weight.shape, BF16),
            pltpu.VMEM((1, d), F32),
            pltpu.VMEM((own_n, d), BF16),
        ),
        in_specs=[hbm] * 13,
        out_specs=(vmem,) * 4,
        scratch_shapes=[
            pltpu.VMEM((tokens, d), BF16),
            pltpu.VMEM((c_here, d), BF16),
            pltpu.VMEM((kt, d), BF16),
            pltpu.VMEM((kt, d), BF16),
            pltpu.VMEM((kt, d), BF16),
            pltpu.VMEM((d, 3 * width), BF16),
            pltpu.VMEM((nt, 8, d // 2), F32),
            pltpu.VMEM((nt, 8, d // 8), F32),
            pltpu.VMEM((8, d), F32),
            pltpu.VMEM((tokens, HEAD_DIM), F32),
            pltpu.VMEM((2, UP_ROWS * GRID_W, d), BF16),
            pltpu.VMEM((ny, ns // ny, c_here, 2 * width), BF16),
            pltpu.VMEM((tokens + halo, 2 * width), BF16),
            pltpu.VMEM((tokens, width), BF16),
            pltpu.VMEM((heads, TABLES + 3, GRID_W, PAIR), F32),
            pltpu.VMEM((heads, tokens, KEYS), F32),
            pltpu.VMEM((heads, tokens, ns // ny * c_here), F32),
            pltpu.VMEM((heads, tokens, 2 * HEAD_DIM), F32),
            pltpu.VMEM((heads, tokens, HEAD_DIM), F32),
            pltpu.VMEM((tokens, width), BF16),
            pltpu.VMEM((2 * WIN_ROWS - 1, heads, PAIR), F32),
            pltpu.VMEM((1, d), F32),
            pltpu.VMEM((1, d), F32),
            pltpu.VMEM((1, d), F32),
            pltpu.VMEM(table.shape, F32),
            sem((12 + 4 * (d // 2 // 512),)),
            sem((nt,)), sem((nt,)), sem((nt,)), sem((nt,)),
            sem((ny + 1, ns // ny)), sem((ns,)),
            sem((2,)), sem((2,)),
            sem((nt,)), sem((nt,)),
        ],
        compiler_params=pltpu.CompilerParams(
            collective_id=0, has_side_effects=True, vmem_limit_bytes=VMEM_BYTES - tail
        ),
    )(
        cond[None], ctx_cond[None], norm_gain[None], table, latents, context, shift_weight, scale_weight, gate_weight,
        q_weight, k_weight, v_weight, out_weight,
    )
    return pl.pallas_call(
        finish,
        out_shape=jax.ShapeDtypeStruct((own_n, d), BF16),
        in_specs=[vmem] * 4,
        out_specs=hbm,
        scratch_shapes=[pltpu.VMEM((own_n, d), BF16), sem((4,))],
        compiler_params=pltpu.CompilerParams(vmem_limit_bytes=16 * 1024 * 1024),
    )(*parts)


def solution(mesh):
    in_specs = (
        P("sp", None),
        P(),
        P(),
        P("sp", None),
        P(),
        P("tp", None),
        P("tp", None),
        P("tp", None),
        P(None, "tp"),
        P(None, "tp"),
        P(None, "tp"),
        P(),
        P("tp", None, None),
    )
    body = functools.partial(shards, mesh.shape["sp"], mesh.shape["tp"])
    return jax.shard_map(
        body, mesh=mesh, in_specs=in_specs, out_specs=P(("sp", "tp"), None), check_vma=False
    )
```

time: 39.1 us -> 36.1 us (0.923)
  local copies, waits for them, and re-layouts: 1.98 us -> 0 us
  Pallas kernels: 36.8 us -> 35.8 us
    unnamed x1 -> x0, local copies, waits for them, and re-layouts: 1.98 us -> none
    pallas_call x1 -> x2, Pallas kernels: 36.8 us -> 35.8 us  [the longest x1 34.2 us: shards(): pl.pallas_call(functools.partial(kernel, ns, nt, ny), out_shape=(pltpu.VM...]
where the time goes in v1:
time: 36.1 us; the launch traced here: 35.8 us
  Pallas kernels  35.8 us (99%)
    pallas_call x1, Pallas kernels, shards(): pl.pallas_call(functools.partial(kernel, ns, nt, ny), out_shape=(pltpu.VM...  34.2 us
    pallas_call x1, Pallas kernels, shards(): pl.pallas_call(finish, out_shape=jax.ShapeDtypeStruct((own_n, d), BF16),...  1.6 us

profile of v1, /device:TPU:1, one launch (start us, length us, event | category | flops | bytes accessed | tf_op | source)
XLA Modules:
  0.0 35.8 jit_solution(2468486890926365461)
XLA Ops:
  0.0 34.2 %shard_map.127 = (bf16[4,160,256]{2,1,0:T(8,128)(2,1)S(1)}, bf16[1024,2048]{1,0:T(8,128)(2,1)S(1)}, f32[1,2048]{1,0:T(1,128)S(1)}, bf16[160,2048]{1,0:T(8,128)(2,1)S(1)}) custom-call(f32[1,2048]{1,0:T(1,128)} %bitcast.5, f32[1,2048]{1,0:T(1,128)} %bitcast.6, f32[1,2048]{1,0:T(1,128)} %bitcast.7, f32[15,2,31]{2,1,0:T(2,128)} %bitcast.4, ...), custom_call_target="tpu_custom_call" | custom-call | tf_op jit(solution)/shard_map/pallas_call | solution.py:541
  34.2 1.6 %shard_map.128 = bf16[160,2048]{1,0:T(8,128)(2,1)} custom-call(bf16[4,160,256]{2,1,0:T(8,128)(2,1)S(1)} %get-tuple-element.9.own, bf16[1024,2048]{1,0:T(8,128)(2,1)S(1)} %get-tuple-element.10.wo, f32[1,2048]{1,0:T(1,128)S(1)} %get-tuple-element.11.gates, bf16[160,2048]{1,0:T(8,128)(2,1)S(1)} %get-tuple-element.12.lat_own), custom_call_target="tpu_custom_call" | custom-call | tf_op jit(solution)/shard_map/pallas_call | solution.py:590

commit v2 on v1

--- a/solution.py
+++ b/solution.py
@@ -21,6 +21,11 @@
 KEY_ROWS = WIN_ROWS + 2
 KEYS = KEY_ROWS * GRID_W
 TABLES = 2 * WIN_ROWS - 2
+Z_FIRST = 3
+HALO = ((0, 2), (2, 1))
+ISSUE = ((), (0,), (1,))
+RAW_PARTS = 2
+CORES = 2
 VMEM_BYTES = 67043328
 
 
@@ -33,9 +38,7 @@
 
 
 def wide(x, n):
-    if n % HEAD_DIM:
-        return x[:, 0:1]
-    return jnp.concatenate([x] * (n // HEAD_DIM), axis=1)
+    return jnp.concatenate([x] * pl.cdiv(n, HEAD_DIM), axis=1)[:, :n]
 
 
 def kernel(
@@ -44,9 +47,9 @@
     lat_h, ctx_h, wsh_h, wsc_h, wg_h, wq_h, wk_h, wv_h, wo_h,
     own, wo, gates, lat_own,
     lat, ctx, wsh, wsc, wg, wqkv,
-    modr, gater, mods, inv, hbuf, ctx_all, kv, q, bias, s_near, s_far, acc, mx, att, lines,
+    modr, gater, mods, inv, hbuf, ctx_all, kv, q, raw, bias, s_near, s_far, acc, mx, att, lines,
     cond, ctx_cond, gain, table,
-    load_sem, mod_s, mod_r, gate_s, gate_r, ctx_s, ctx_r, halo_s, halo_r, head_s, head_r,
+    load_sem, mod_s, mod_r, gate_s, gate_r, across_s, along_s, ctx_r, halo_s, halo_r, raw_s, raw_r, head_s, head_r,
 ):
     sp, tp = lax.axis_index("sp"), lax.axis_index("tp")
     tokens, d = lat.shape
@@ -84,7 +87,7 @@
     wo_load = load(wo_h, wo)
     my_rows = pl.ds(pl.multiple_of(tp * own_n, 16), own_n)
     own_load = load(lat_h.at[my_rows], lat_own)
-    for c in small + sum(mod_loads, []) + [ctx_load, lat_load, wg_load, wk_load, wv_load, wq_load, wo_load, own_load]:
+    for c in small + sum(mod_loads, []) + [ctx_load, lat_load]:
         c.start()
 
     barrier = pltpu.get_barrier_semaphore()
@@ -118,29 +121,106 @@
 
     a_sh = [only(mixed_act, (row // 2) == 2 * k) for k in range(2)]
     a_sc = [only(mixed_act, (row // 2) == 2 * k + 1) for k in range(2)]
-    for i, n0 in enumerate(range(0, half_d, step)):
+    def mod_copy(i, o):
+        return pltpu.make_async_remote_copy(
+            src_ref=modr.at[i, tp], dst_ref=modr.at[i, tp],
+            send_sem=mod_s.at[i, o - 1], recv_sem=mod_r.at[i, o - 1],
+            device_id={"sp": sp, "tp": (tp + o) % nt},
+        )
+
+    def each_mod(i, act):
+        def one(o, _):
+            act(mod_copy(i, o))
+            return 0
+
+        lax.fori_loop(1, nt, one, 0)
+
+    chunks = half_d // step
+    for i in range(chunks):
         part = jnp.zeros((8, step), F32)
         for k in range(2):
-            cols = pl.ds(k * half_d + n0, step)
+            cols = pl.ds(k * half_d + i * step, step)
             mod_loads[i][2 * k].wait()
             part = part + dot(a_sh[k], wsh[:, cols])
             mod_loads[i][2 * k + 1].wait()
             part = part + dot(a_sc[k], wsc[:, cols])
-        modr[tp, :, pl.ds(n0, step)] = part
-    pl.semaphore_wait(barrier, nt - 1 + ns - 1)
+        modr[i, tp] = part.astype(BF16)
+        if i == 0:
+            pl.semaphore_wait(barrier, nt - 1 + ns - 1)
+        each_mod(i, lambda c: c.start())
+    quarter = up_n // nt
+    piece = quarter // RAW_PARTS
+    nx = nt // CORES
+    core, xi = tp % CORES, tp // CORES
+    has_next, has_prev = sp < ns - 1, sp > 0
+
+    def raw_at(i, t):
+        return raw.at[pl.ds(pl.multiple_of(t * quarter, 16) + i * piece, piece)]
+
+    def raw_first(i):
+        src = lat_h.at[pl.ds(pl.multiple_of(tokens - up_n + tp * quarter, 16) + i * piece, piece)]
+        return pltpu.make_async_remote_copy(
+            src_ref=src, dst_ref=raw_at(i, tp), send_sem=raw_s.at[i, 0], recv_sem=raw_r.at[i, tp],
+            device_id={"sp": (sp + 1) % ns, "tp": tp},
+        )
+
+    def raw_next(i, t, dest, lane):
+        return pltpu.make_async_remote_copy(
+            src_ref=raw_at(i, t), dst_ref=raw_at(i, t), send_sem=raw_s.at[i, lane], recv_sem=raw_r.at[i, t],
+            device_id={"sp": sp, "tp": dest},
+        )
+
+    def raw_x(i, o):
+        return raw_next(i, tp, (xi + o) % nx * CORES + core, o)
+
+    def raw_mate(i, o):
+        return raw_next(i, (xi + o) % nx * CORES + core, xi * CORES + (core + 1) % CORES, nx + o)
+
+    def raw_got(i, t):
+        raw_next(i, t, tp, 0).wait_recv()
+
+    def raw_along(i):
+        @pl.when(has_prev)
+        def _():
+            raw_got(i, tp)
+            for o in range(1, nx):
+                raw_x(i, o).start()
+            raw_mate(i, 0).start()
+
+    def raw_over(i):
+        @pl.when(has_prev)
+        def _():
+            for o in range(1, nx):
+                raw_got(i, (xi + o) % nx * CORES + core)
+                raw_mate(i, o).start()
+
+    def raw_done(i):
+        @pl.when(has_next)
+        def _():
+            raw_first(i).wait_send()
+
+        @pl.when(has_prev)
+        def _():
+            for o in range(nx):
+                raw_got(i, (xi + o) % nx * CORES + (core + 1) % CORES)
+                raw_mate(i, o).wait_send()
+                if o:
+                    raw_x(i, o).wait_send()
+
+    @pl.when(has_next)
+    def _():
+        for i in range(RAW_PARTS):
+            raw_first(i).start()
+
+    for c in [wg_load, wk_load, wv_load, wq_load, wo_load, own_load]:
+        c.start()
 
     def tp_copy(buf, s_sem, r_sem, o):
         return pltpu.make_async_remote_copy(
             src_ref=buf.at[tp], dst_ref=buf.at[tp],
-            send_sem=s_sem.at[o], recv_sem=r_sem.at[o],
+            send_sem=s_sem.at[o - 1], recv_sem=r_sem.at[o - 1],
             device_id={"sp": sp, "tp": (tp + o) % nt},
         )
-
-    def start_mod(o, _):
-        tp_copy(modr, mod_s, mod_r, o).start()
-        return 0
-
-    lax.fori_loop(1, nt, start_mod, 0)
 
     qc = lax.broadcasted_iota(jnp.int32, (GRID_W, PAIR), 0)
     lane = lax.broadcasted_iota(jnp.int32, (GRID_W, PAIR), 1)
@@ -170,7 +250,7 @@
 
     @pl.when(sp == 0)
     def _():
-        kv[0:up_n, :] = jnp.zeros((up_n, 2 * width), BF16)
+        raw[...] = jnp.zeros_like(raw)
 
     @pl.when(sp == ns - 1)
     def _():
@@ -203,22 +283,21 @@
     wk_load.wait()
     wv_load.wait()
 
-    def wait_mod(o, _):
-        tp_copy(modr, mod_s, mod_r, o).wait()
-        return 0
-
-    lax.fori_loop(1, nt, wait_mod, 0)
-    total = modr[0]
-    for i in range(1, nt):
-        total = total + modr[i]
+    for i in range(chunks):
+        each_mod(i, lambda c: c.wait())
     g = gain[...]
-    for k in range(2):
-        cols = pl.ds(k * half_d, half_d)
-        gk = g[:, k * half_d:(k + 1) * half_d]
-        mods[0:1, cols] = gk * (1.0 + total[4 * k + 2:4 * k + 3])
-        mods[1:2, cols] = total[4 * k:4 * k + 1]
-        mods[2:3, cols] = gk * (1.0 + total[4 * k + 3:4 * k + 4])
-        mods[3:4, cols] = total[4 * k + 1:4 * k + 2]
+    for i in range(chunks):
+        total = modr[i, 0].astype(F32)
+        for j in range(1, nt):
+            total = total + modr[i, j].astype(F32)
+        for k in range(2):
+            lo = k * half_d + i * step
+            cols = pl.ds(lo, step)
+            gk = g[:, lo:lo + step]
+            mods[0:1, cols] = gk * (1.0 + total[4 * k + 2:4 * k + 3])
+            mods[1:2, cols] = total[4 * k:4 * k + 1]
+            mods[2:3, cols] = gk * (1.0 + total[4 * k + 3:4 * k + 4])
+            mods[3:4, cols] = total[4 * k + 1:4 * k + 2]
 
     ctx_hid = (ctx[...].astype(F32) * ctx_inv * mods[2:3, :] + mods[3:4, :]).astype(BF16)
     ctx_all[sp % ny, sp // ny] = dot(ctx_hid, wqkv[:, 0:2 * width]).astype(BF16)
@@ -226,30 +305,35 @@
     nz = ns // ny
     zi, yi = sp // ny, sp % ny
 
-    def ctx_copy(block, dest, lane):
+    cut = max(Z_FIRST * width // 2 // HEAD_DIM, 1) * HEAD_DIM
+
+    def ctx_copy(part, block, dest, send_sem):
+        cols = pl.ds(0, cut) if part == 0 else pl.ds(cut, 2 * width - cut)
+        ref = ctx_all.at[block % ny, block // ny, :, cols]
         return pltpu.make_async_remote_copy(
-            src_ref=ctx_all.at[block % ny, block // ny],
-            dst_ref=ctx_all.at[block % ny, block // ny],
-            send_sem=ctx_s.at[lane, block // ny], recv_sem=ctx_r.at[block],
+            src_ref=ref, dst_ref=ref, send_sem=send_sem, recv_sem=ctx_r.at[part, block],
             device_id={"sp": dest, "tp": tp},
         )
 
-    def across(zb, act):
+    def slot(part, block):
+        return block + nz if part else block // ny
+
+    def across(part, zb, act):
         def one(o, _):
-            act(ctx_copy(zb * ny + yi, zi * ny + (yi + o) % ny, 1 + o))
+            act(ctx_copy(part, zb * ny + yi, zi * ny + (yi + o) % ny, across_s.at[part * nz + zb, o - 1]))
             return 0
 
         lax.fori_loop(1, ny, one, 0)
 
-    def upward(zb, act):
+    def upward(part, block, act):
         @pl.when(zi < nz - 1)
         def _():
-            act(ctx_copy(zb * ny + yi, sp + ny, 0))
-
-    def downward(zb, act):
+            act(ctx_copy(part, block, sp + ny, along_s.at[0, slot(part, block)]))
+
+    def downward(part, block, act):
         @pl.when(zi > 0)
         def _():
-            act(ctx_copy(zb * ny + yi, sp - ny, 1))
+            act(ctx_copy(part, block, sp - ny, along_s.at[1, slot(part, block)]))
 
     def go(c):
         c.start()
@@ -257,46 +341,72 @@
     def sent(c):
         c.wait_send()
 
-    def arrived(block):
-        ctx_copy(block, sp, 0).wait_recv()
-
-    def relay(k):
+    def arrived(part, block):
+        ctx_copy(part, block, sp, along_s.at[0, slot(part, block)]).wait_recv()
+
+    def beside():
+        def one(o, _):
+            block = zi * ny + (yi + o) % ny
+            arrived(1, block)
+            upward(1, block, go)
+            downward(1, block, go)
+            return 0
+
+        lax.fori_loop(1, ny, one, 0)
+
+    def pass_first(zb, forward):
+        block = zb * ny + yi
+        arrived(0, block)
+        forward(0, block, go)
+        across(0, zb, go)
+
+    def pass_second(zb, forward):
+        def one(o, _):
+            other = zb * ny + (yi + o) % ny
+            arrived(1, other)
+            forward(1, other, go)
+            return 0
+
+        lax.fori_loop(0, ny, one, 0)
+
+    def relay(k, pass_on):
+        @pl.when(zi + k < nz)
+        def _():
+            pass_on(zi + k, downward)
+
         @pl.when(zi - k >= 0)
         def _():
-            arrived((zi - k) * ny + yi)
-            upward(zi - k, go)
-            across(zi - k, go)
-
-        @pl.when(zi + k < nz)
-        def _():
-            arrived((zi + k) * ny + yi)
-            downward(zi + k, go)
-            across(zi + k, go)
-
-    upward(zi, go)
-    downward(zi, go)
-    across(zi, go)
-
-    up = pltpu.make_async_remote_copy(
-        src_ref=kv.at[pl.ds(tokens, up_n)], dst_ref=kv.at[pl.ds(0, up_n)],
-        send_sem=halo_s.at[0], recv_sem=halo_r.at[0],
-        device_id={"sp": (sp + 1) % ns, "tp": tp},
-    )
-    down = pltpu.make_async_remote_copy(
-        src_ref=kv.at[pl.ds(up_n, down_n)], dst_ref=kv.at[pl.ds(up_n + tokens, down_n)],
-        send_sem=halo_s.at[1], recv_sem=halo_r.at[1],
-        device_id={"sp": (sp + ns - 1) % ns, "tp": tp},
-    )
-    has_next, has_prev = sp < ns - 1, sp > 0
+            pass_on(zi - k, upward)
+
+    across(1, zi, go)
+    for part in range(2):
+        upward(part, sp, go)
+        downward(part, sp, go)
+    across(0, zi, go)
+
+    def halo(i):
+        lo, n = HALO[i]
+        return pltpu.make_async_remote_copy(
+            src_ref=kv.at[pl.ds(up_n + lo * GRID_W, n * GRID_W)],
+            dst_ref=kv.at[pl.ds(up_n + tokens + lo * GRID_W, n * GRID_W)],
+            send_sem=halo_s.at[i], recv_sem=halo_r.at[i],
+            device_id={"sp": (sp + ns - 1) % ns, "tp": tp},
+        )
+
+    def send_halo(point):
+        for i in ISSUE[point]:
+            pl.when(has_prev)(lambda c=halo(i): c.start())
 
     wq_load.wait()
-    spans = [(tokens - up_n, up_n), (0, down_n), (down_n, tokens - up_n - down_n)]
+    rest = (tokens - down_n) // 2
+    spans = [(0, down_n), (down_n, rest), (down_n + rest, rest)]
+
+    def modulate(x, scale):
+        return (x.astype(F32) * scale * mods[0:1, :] + mods[1:2, :]).astype(BF16)
 
     def hidden(i):
         lo, n = spans[i]
-        x = lat[lo:lo + n, :].astype(F32)
-        h = x * wide(inv[lo:lo + n, :], d) * mods[0:1, :] + mods[1:2, :]
-        hbuf[i % 2, 0:n, :] = h.astype(BF16)
+        hbuf[i % 2, 0:n, :] = modulate(lat[lo:lo + n, :], wide(inv[lo:lo + n, :], d))
 
     hidden(0)
     for i, (lo, n) in enumerate(spans):
@@ -306,9 +416,11 @@
         if i + 1 < len(spans):
             hidden(i + 1)
         if i == 0:
-            pl.when(has_next)(lambda: up.start())
+            send_halo(0)
+            raw_along(0)
         if i == 1:
-            pl.when(has_prev)(lambda: down.start())
+            beside()
+            send_halo(1)
 
     half_t = nt // 2
     my_half = tp // half_t
@@ -368,91 +480,128 @@
             near_values(r, h, m)
 
     def flat(x):
+        n = x.shape[0] * c_here
         if c_here % 16:
-            return x.astype(F32).reshape(nz * c_here, HEAD_DIM).astype(BF16)
-        return x.reshape(nz * c_here, HEAD_DIM)
-
-    far_n = nz * c_here
-
-    def far_scores(t, col, h):
+            return x.astype(F32).reshape(n, HEAD_DIM).astype(BF16)
+        return x.reshape(n, HEAD_DIM)
+
+    def far_scores(t, col, zs, h):
         lo = h * HEAD_DIM
-        s = dot_t(q[t, lo:lo + HEAD_DIM], flat(ctx_all[col, :, :, lo:lo + HEAD_DIM]))
-        s_far[h, t, :] = s
+        s = dot_t(q[t, lo:lo + HEAD_DIM], flat(ctx_all[col, zs, :, lo:lo + HEAD_DIM]))
+        s_far[h, t, 0:s.shape[1]] = s
         return jnp.broadcast_to(jnp.max(s, axis=-1, keepdims=True), (own_n, HEAD_DIM))
 
-    def far_values(t, col, h, m, last):
-        lo = h * HEAD_DIM
+    def far_values(t, col, zs, h, m, last):
+        lo = width + h * HEAD_DIM
+        v = flat(ctx_all[col, zs, :, lo:lo + HEAD_DIM])
         old = mx[h, t, :]
         m = jnp.maximum(m, old)
         w = jnp.exp2(old - m)
-        e = jnp.exp2(s_far[h, t, :] - wide(m, far_n)).astype(BF16)
-        o = dot(e, with_ones(flat(ctx_all[col, :, :, width + lo:width + lo + HEAD_DIM])))
-        o = acc[h, t, :] * wide(w, 2 * HEAD_DIM) + o
+        n = v.shape[0]
+        e = jnp.exp2(s_far[h, t, 0:n] - wide(m, n)).astype(BF16)
+        o = acc[h, t, :] * wide(w, 2 * HEAD_DIM) + dot(e, with_ones(v))
         if last:
+            lo = h * HEAD_DIM
             att[t, lo:lo + HEAD_DIM] = (o[:, :HEAD_DIM] / o[:, HEAD_DIM:]).astype(BF16)
         else:
             mx[h, t, :] = m
             acc[h, t, :] = o
 
-    def far(parts, o, last):
+    def far(parts, o, zs, last):
         col = (yi + o) % ny
         units = [(pl.ds(pl.multiple_of(p * own_n, 16), own_n), h) for p in parts for h in range(heads)]
-        ms = [far_scores(t, col, h) for t, h in units]
+        ms = [far_scores(t, col, zs, h) for t, h in units]
         for (t, h), m in zip(units, ms):
-            far_values(t, col, h, m, last)
+            far_values(t, col, zs, h, m, last)
+
+    everything = pl.ds(0, nz)
 
     def far_all(o, _):
-        far(range(nt), o, False)
+        far(range(nt), o, everything, False)
         return 0
 
+    relay(1, pass_first)
+    for i in range(1, RAW_PARTS):
+        raw_along(i)
     near(range(UP_ROWS, rows - UP_ROWS, 2))
-    relay(1)
+    relay(1, pass_second)
+    send_halo(2)
+    raw_over(0)
     if nz > 2:
-        relay(2)
+        relay(2, pass_first)
+    if nz > 2:
+        relay(2, pass_second)
+    for i in range(1, RAW_PARTS):
+        raw_over(i)
+    for i in range(RAW_PARTS):
+        raw_done(i)
+    hbuf[0] = modulate(raw[...], inv_of(raw[...]))
+    kv[0:up_n, :] = dot(hbuf[0], wqkv[:, 0:2 * width]).astype(BF16)
+    near(range(0, UP_ROWS, 2))
     if nz > 3:
-        relay(3)
+        relay(3, pass_first)
+    for i in range(len(HALO)):
+        pl.when(has_prev)(lambda c=halo(i): c.wait_send())
+        pl.when(has_next)(lambda c=halo(i): c.wait_recv())
+
+    near(range(rows - UP_ROWS, rows, 2))
+
+    if nz > 3:
+        relay(3, pass_second)
 
     def late_relay(k, _):
-        relay(k)
+        relay(k, pass_first)
+        relay(k, pass_second)
         return 0
 
     lax.fori_loop(4, nz, late_relay, 0)
+    low = zi < nz - nz // 2
+    z_last = jnp.where(low, nz - 1, 0)
+    z_rest = pl.ds(jnp.where(low, 0, 1), nz - 1)
+
+    def others(zb):
+        def other(o, _):
+            arrived(0, zb * ny + (yi + o) % ny)
+            return 0
+
+        lax.fori_loop(1, ny, other, 0)
+
     if ny > 1:
         far_all(0, 0)
-
-    @pl.when(has_next)
-    def _():
-        down.wait_recv()
-        up.wait_send()
-
-    @pl.when(has_prev)
-    def _():
-        up.wait_recv()
-        down.wait_send()
-
-    near([*range(0, UP_ROWS, 2), *range(rows - UP_ROWS, rows, 2)])
+    for k in range(nz - 1):
+        others(z_rest.start + k)
+    lax.fori_loop(1, ny - 1, lambda o, c: (far(range(nt), o, z_rest, False), c)[1], 0)
+    if nz > 1:
+        far(range(nt), ny - 1, z_rest, False)
+    others(z_last)
+    lax.fori_loop(1, ny - 1, lambda o, c: (far(range(nt), o, pl.ds(z_last, 1), False), c)[1], 0)
 
     def settle_row(zb, _):
-        def other(o, _):
-            arrived(zb * ny + (yi + o) % ny)
+        across(0, zb, sent)
+
+        @pl.when(zb <= zi)
+        def _():
+            upward(0, zb * ny + yi, sent)
+
+        @pl.when(zb >= zi)
+        def _():
+            downward(0, zb * ny + yi, sent)
+
+        def column(o, _):
+            block = zb * ny + o
+
+            @pl.when(zb <= zi)
+            def _():
+                upward(1, block, sent)
+
+            @pl.when(zb >= zi)
+            def _():
+                downward(1, block, sent)
+
             return 0
 
-        lax.fori_loop(1, ny, other, 0)
-        across(zb, sent)
-
-        @pl.when(zb <= zi)
-        def _():
-            upward(zb, sent)
-
-        @pl.when(zb >= zi)
-        def _():
-            downward(zb, sent)
-
+        lax.fori_loop(0, ny, column, 0)
         return 0
-
-    lax.fori_loop(0, nz, settle_row, 0)
-
-    lax.fori_loop(1, ny - 1, far_all, 0)
 
     def head_copy(src, dst):
         return pltpu.make_async_remote_copy(
@@ -461,24 +610,16 @@
             device_id={"sp": sp, "tp": dst},
         )
 
-    other_half = (1 - my_half) * half_t
-    far([other_half + j for j in range(half_t)], ny - 1, True)
-
-    def send_other(j, _):
-        head_copy(tp, (1 - my_half) * half_t + j).start()
-        return 0
-
-    lax.fori_loop(0, half_t, send_other, 0)
-    far([my_half * half_t + j for j in range(half_t)], ny - 1, True)
-
-    def mate(o):
-        return my_half * half_t + (tp + o) % half_t
-
-    def send_same(o, _):
-        head_copy(tp, mate(o)).start()
-        return 0
-
-    lax.fori_loop(1, half_t, send_same, 0)
+    theirs = [(1 - my_half) * half_t + j for j in range(half_t)]
+    ours = [my_half * half_t + (tp + o) % half_t for o in range(half_t)]
+    for p in theirs:
+        far([p], ny - 1, pl.ds(z_last, 1), True)
+        head_copy(tp, p).start()
+    far(ours, ny - 1, pl.ds(z_last, 1), True)
+    for p in ours[1:]:
+        head_copy(tp, p).start()
+    across(1, zi, sent)
+    lax.fori_loop(0, nz, settle_row, 0)
 
     def wait_gate(o, _):
         tp_copy(gater, gate_s, gate_r, o).wait()
@@ -555,7 +696,7 @@
             pltpu.VMEM((kt, d), BF16),
             pltpu.VMEM((kt, d), BF16),
             pltpu.VMEM((d, 3 * width), BF16),
-            pltpu.VMEM((nt, 8, d // 2), F32),
+            pltpu.VMEM((d // 2 // 512, nt, 8, 512), BF16),
             pltpu.VMEM((nt, 8, d // 8), F32),
             pltpu.VMEM((8, d), F32),
             pltpu.VMEM((tokens, HEAD_DIM), F32),
@@ -563,6 +704,7 @@
             pltpu.VMEM((ny, ns // ny, c_here, 2 * width), BF16),
             pltpu.VMEM((tokens + halo, 2 * width), BF16),
             pltpu.VMEM((tokens, width), BF16),
+            pltpu.VMEM((UP_ROWS * GRID_W, d), BF16),
             pltpu.VMEM((heads, TABLES + 3, GRID_W, PAIR), F32),
             pltpu.VMEM((heads, tokens, KEYS), F32),
             pltpu.VMEM((heads, tokens, ns // ny * c_here), F32),
@@ -575,9 +717,10 @@
             pltpu.VMEM((1, d), F32),
             pltpu.VMEM(table.shape, F32),
             sem((12 + 4 * (d // 2 // 512),)),
-            sem((nt,)), sem((nt,)), sem((nt,)), sem((nt,)),
-            sem((ny + 1, ns // ny)), sem((ns,)),
-            sem((2,)), sem((2,)),
+            sem((d // 2 // 512, nt - 1)), sem((d // 2 // 512, nt - 1)), sem((nt - 1,)), sem((nt - 1,)),
+            sem((2 * (ns // ny), max(ny - 1, 1))), sem((2, ns + ns // ny)), sem((2, ns)),
+            sem((len(HALO),)), sem((len(HALO),)),
+            sem((RAW_PARTS, 2 * (nt // CORES))), sem((RAW_PARTS, nt)),
             sem((nt,)), sem((nt,)),
         ],
         compiler_params=pltpu.CompilerParams(

time: 36.1 us -> 35.6 us (0.986)
  Pallas kernels: 35.8 us -> 35.2 us
    pallas_call x1, Pallas kernels: 34.2 us -> 33.6 us  [shards(): pl.pallas_call(functools.partial(kernel, ns, nt, ny), out_shape=(pltpu.VM...]
where the time goes in v2:
time: 35.6 us; the launch traced here: 35.4 us
  Pallas kernels  35.2 us (99%)
    pallas_call x1, Pallas kernels, shards(): pl.pallas_call(functools.partial(kernel, ns, nt, ny), out_shape=(pltpu.VM...  33.6 us
    pallas_call x1, Pallas kernels, shards(): pl.pallas_call(finish, out_shape=jax.ShapeDtypeStruct((own_n, d), BF16),...  1.6 us

profile of v2, /device:TPU:1, one launch (start us, length us, event | category | flops | bytes accessed | tf_op | source)
XLA Modules:
  0.0 35.4 jit_solution(5205156317580440118)
XLA Ops:
  0.0 33.6 %shard_map.127 = (bf16[4,160,256]{2,1,0:T(8,128)(2,1)S(1)}, bf16[1024,2048]{1,0:T(8,128)(2,1)S(1)}, f32[1,2048]{1,0:T(1,128)S(1)}, bf16[160,2048]{1,0:T(8,128)(2,1)S(1)}) custom-call(f32[1,2048]{1,0:T(1,128)} %bitcast.5, f32[1,2048]{1,0:T(1,128)} %bitcast.6, f32[1,2048]{1,0:T(1,128)} %bitcast.7, f32[15,2,31]{2,1,0:T(2,128)} %bitcast.4, ...), custom_call_target="tpu_custom_call" | custom-call | tf_op jit(solution)/shard_map/pallas_call | solution.py:682
  33.6 1.6 %shard_map.128 = bf16[160,2048]{1,0:T(8,128)(2,1)} custom-call(bf16[4,160,256]{2,1,0:T(8,128)(2,1)S(1)} %get-tuple-element.9.own, bf16[1024,2048]{1,0:T(8,128)(2,1)S(1)} %get-tuple-element.10.wo, f32[1,2048]{1,0:T(1,128)S(1)} %get-tuple-element.11.gates, bf16[160,2048]{1,0:T(8,128)(2,1)S(1)} %get-tuple-element.12.lat_own), custom_call_target="tpu_custom_call" | custom-call | tf_op jit(solution)/shard_map/pallas_call | solution.py:733

commit v3 on v2

--- a/solution.py
+++ b/solution.py
@@ -22,9 +22,9 @@
 KEYS = KEY_ROWS * GRID_W
 TABLES = 2 * WIN_ROWS - 2
 Z_FIRST = 3
-HALO = ((0, 2), (2, 1))
-ISSUE = ((), (0,), (1,))
-RAW_PARTS = 2
+HALO = ((0, 2), (2, 2))
+ISSUE = ((), (0,), (), (1,))
+RAW_PARTS = 1
 CORES = 2
 VMEM_BYTES = 67043328
 
@@ -68,16 +68,20 @@
 
     count = [0]
 
-    def load(s, t):
-        c = pltpu.make_async_copy(s, t, load_sem.at[count[0]])
+    def load(s, t, same=None):
+        if same is None:
+            same = count[0]
+            count[0] += 1
+        return pltpu.make_async_copy(s, t, load_sem.at[same])
+
+    small = [load(cond_h, cond), load(ctx_cond_h, ctx_cond), load(gain_h, gain), load(table_h, table)]
+    mod_loads, mod_slots = [], []
+    for n0 in range(0, half_d, step):
+        slot_here = count[0]
+        mod_slots.append(slot_here)
         count[0] += 1
-        return c
-
-    small = [load(cond_h, cond), load(ctx_cond_h, ctx_cond), load(gain_h, gain), load(table_h, table)]
-    mod_loads = []
-    for n0 in range(0, half_d, step):
         mod_loads.append([
-            load(s.at[:, pl.ds(k * half_d + n0, step)], t.at[:, pl.ds(k * half_d + n0, step)])
+            load(s.at[:, pl.ds(k * half_d + n0, step)], t.at[:, pl.ds(k * half_d + n0, step)], slot_here)
             for k in range(2) for s, t in ((wsh_h, wsh), (wsc_h, wsc))
         ])
     ctx_load, lat_load, wg_load = load(ctx_h, ctx), load(lat_h, lat), load(wg_h, wg)
@@ -124,7 +128,7 @@
     def mod_copy(i, o):
         return pltpu.make_async_remote_copy(
             src_ref=modr.at[i, tp], dst_ref=modr.at[i, tp],
-            send_sem=mod_s.at[i, o - 1], recv_sem=mod_r.at[i, o - 1],
+            send_sem=mod_s.at[o - 1], recv_sem=mod_r.at[o - 1],
             device_id={"sp": sp, "tp": (tp + o) % nt},
         )
 
@@ -137,31 +141,30 @@
 
     chunks = half_d // step
     for i in range(chunks):
+        load(wsh_h.at[:, pl.ds(0, 4 * step)], wsh.at[:, pl.ds(0, 4 * step)], mod_slots[i]).wait()
         part = jnp.zeros((8, step), F32)
         for k in range(2):
             cols = pl.ds(k * half_d + i * step, step)
-            mod_loads[i][2 * k].wait()
             part = part + dot(a_sh[k], wsh[:, cols])
-            mod_loads[i][2 * k + 1].wait()
             part = part + dot(a_sc[k], wsc[:, cols])
-        modr[i, tp] = part.astype(BF16)
+        modr[i, tp] = part
         if i == 0:
             pl.semaphore_wait(barrier, nt - 1 + ns - 1)
         each_mod(i, lambda c: c.start())
-    quarter = up_n // nt
+    quarter = down_n // nt
     piece = quarter // RAW_PARTS
     nx = nt // CORES
     core, xi = tp % CORES, tp // CORES
     has_next, has_prev = sp < ns - 1, sp > 0
 
     def raw_at(i, t):
-        return raw.at[pl.ds(pl.multiple_of(t * quarter, 16) + i * piece, piece)]
+        return raw.at[pl.ds(pl.multiple_of(t * quarter, 8) + i * piece, piece)]
 
     def raw_first(i):
-        src = lat_h.at[pl.ds(pl.multiple_of(tokens - up_n + tp * quarter, 16) + i * piece, piece)]
+        src = lat_h.at[pl.ds(pl.multiple_of(tp * quarter, 8) + i * piece, piece)]
         return pltpu.make_async_remote_copy(
             src_ref=src, dst_ref=raw_at(i, tp), send_sem=raw_s.at[i, 0], recv_sem=raw_r.at[i, tp],
-            device_id={"sp": (sp + 1) % ns, "tp": tp},
+            device_id={"sp": (sp + ns - 1) % ns, "tp": tp},
         )
 
     def raw_next(i, t, dest, lane):
@@ -180,7 +183,7 @@
         raw_next(i, t, tp, 0).wait_recv()
 
     def raw_along(i):
-        @pl.when(has_prev)
+        @pl.when(has_next)
         def _():
             raw_got(i, tp)
             for o in range(1, nx):
@@ -188,18 +191,18 @@
             raw_mate(i, 0).start()
 
     def raw_over(i):
-        @pl.when(has_prev)
+        @pl.when(has_next)
         def _():
             for o in range(1, nx):
                 raw_got(i, (xi + o) % nx * CORES + core)
                 raw_mate(i, o).start()
 
     def raw_done(i):
+        @pl.when(has_prev)
+        def _():
+            raw_first(i).wait_send()
+
         @pl.when(has_next)
-        def _():
-            raw_first(i).wait_send()
-
-        @pl.when(has_prev)
         def _():
             for o in range(nx):
                 raw_got(i, (xi + o) % nx * CORES + (core + 1) % CORES)
@@ -207,7 +210,7 @@
                 if o:
                     raw_x(i, o).wait_send()
 
-    @pl.when(has_next)
+    @pl.when(has_prev)
     def _():
         for i in range(RAW_PARTS):
             raw_first(i).start()
@@ -248,13 +251,13 @@
     acc[...] = jnp.zeros_like(acc)
     n_keys = kv.shape[0] - tokens - up_n
 
+    @pl.when(sp == ns - 1)
+    def _():
+        raw[...] = jnp.zeros_like(raw)
+
     @pl.when(sp == 0)
     def _():
-        raw[...] = jnp.zeros_like(raw)
-
-    @pl.when(sp == ns - 1)
-    def _():
-        kv[pl.ds(up_n + tokens, down_n), :] = jnp.zeros((down_n, 2 * width), BF16)
+        kv[0:up_n, :] = jnp.zeros((up_n, 2 * width), BF16)
 
     kv[pl.ds(up_n + tokens + down_n, n_keys - down_n), :] = jnp.zeros((n_keys - down_n, 2 * width), BF16)
 
@@ -283,13 +286,12 @@
     wk_load.wait()
     wv_load.wait()
 
-    for i in range(chunks):
-        each_mod(i, lambda c: c.wait())
+    each_mod(pl.ds(0, chunks), lambda c: c.wait())
     g = gain[...]
     for i in range(chunks):
-        total = modr[i, 0].astype(F32)
+        total = modr[i, 0]
         for j in range(1, nt):
-            total = total + modr[i, j].astype(F32)
+            total = total + modr[i, j]
         for k in range(2):
             lo = k * half_d + i * step
             cols = pl.ds(lo, step)
@@ -308,19 +310,16 @@
     cut = max(Z_FIRST * width // 2 // HEAD_DIM, 1) * HEAD_DIM
 
     def ctx_copy(part, block, dest, send_sem):
-        cols = pl.ds(0, cut) if part == 0 else pl.ds(cut, 2 * width - cut)
+        cols = (pl.ds(0, cut), pl.ds(cut, 2 * width - cut), pl.ds(0, 2 * width))[part]
         ref = ctx_all.at[block % ny, block // ny, :, cols]
         return pltpu.make_async_remote_copy(
-            src_ref=ref, dst_ref=ref, send_sem=send_sem, recv_sem=ctx_r.at[part, block],
+            src_ref=ref, dst_ref=ref, send_sem=send_sem, recv_sem=ctx_r.at[part % 2, block],
             device_id={"sp": dest, "tp": tp},
         )
 
-    def slot(part, block):
-        return block + nz if part else block // ny
-
     def across(part, zb, act):
         def one(o, _):
-            act(ctx_copy(part, zb * ny + yi, zi * ny + (yi + o) % ny, across_s.at[part * nz + zb, o - 1]))
+            act(ctx_copy(part, zb * ny + yi, zi * ny + (yi + o) % ny, across_s.at[zb, o - 1]))
             return 0
 
         lax.fori_loop(1, ny, one, 0)
@@ -328,12 +327,12 @@
     def upward(part, block, act):
         @pl.when(zi < nz - 1)
         def _():
-            act(ctx_copy(part, block, sp + ny, along_s.at[0, slot(part, block)]))
+            act(ctx_copy(part, block, sp + ny, along_s.at[0, block]))
 
     def downward(part, block, act):
         @pl.when(zi > 0)
         def _():
-            act(ctx_copy(part, block, sp - ny, along_s.at[1, slot(part, block)]))
+            act(ctx_copy(part, block, sp - ny, along_s.at[1, block]))
 
     def go(c):
         c.start()
@@ -342,7 +341,7 @@
         c.wait_send()
 
     def arrived(part, block):
-        ctx_copy(part, block, sp, along_s.at[0, slot(part, block)]).wait_recv()
+        ctx_copy(part, block, sp, along_s.at[0, block]).wait_recv()
 
     def beside():
         def one(o, _):
@@ -387,19 +386,19 @@
     def halo(i):
         lo, n = HALO[i]
         return pltpu.make_async_remote_copy(
-            src_ref=kv.at[pl.ds(up_n + lo * GRID_W, n * GRID_W)],
-            dst_ref=kv.at[pl.ds(up_n + tokens + lo * GRID_W, n * GRID_W)],
+            src_ref=kv.at[pl.ds(tokens + lo * GRID_W, n * GRID_W)],
+            dst_ref=kv.at[pl.ds(lo * GRID_W, n * GRID_W)],
             send_sem=halo_s.at[i], recv_sem=halo_r.at[i],
-            device_id={"sp": (sp + ns - 1) % ns, "tp": tp},
+            device_id={"sp": (sp + 1) % ns, "tp": tp},
         )
 
     def send_halo(point):
         for i in ISSUE[point]:
-            pl.when(has_prev)(lambda c=halo(i): c.start())
+            pl.when(has_next)(lambda c=halo(i): c.start())
 
     wq_load.wait()
-    rest = (tokens - down_n) // 2
-    spans = [(0, down_n), (down_n, rest), (down_n + rest, rest)]
+    rest = (tokens - up_n) // 2
+    spans = [(tokens - up_n, up_n), (0, rest), (rest, rest)]
 
     def modulate(x, scale):
         return (x.astype(F32) * scale * mods[0:1, :] + mods[1:2, :]).astype(BF16)
@@ -526,26 +525,21 @@
     near(range(UP_ROWS, rows - UP_ROWS, 2))
     relay(1, pass_second)
     send_halo(2)
-    raw_over(0)
     if nz > 2:
         relay(2, pass_first)
+    send_halo(3)
+    for i in range(RAW_PARTS):
+        raw_over(i)
     if nz > 2:
         relay(2, pass_second)
-    for i in range(1, RAW_PARTS):
-        raw_over(i)
     for i in range(RAW_PARTS):
         raw_done(i)
-    hbuf[0] = modulate(raw[...], inv_of(raw[...]))
-    kv[0:up_n, :] = dot(hbuf[0], wqkv[:, 0:2 * width]).astype(BF16)
-    near(range(0, UP_ROWS, 2))
+    hbuf[0, 0:down_n, :] = modulate(raw[...], inv_of(raw[...]))
+    below = dot(hbuf[0, 0:down_n, :], wqkv[:, 0:2 * width])
+    kv[up_n + tokens:up_n + tokens + down_n, :] = below.astype(BF16)
+    near(range(rows - UP_ROWS, rows, 2))
     if nz > 3:
         relay(3, pass_first)
-    for i in range(len(HALO)):
-        pl.when(has_prev)(lambda c=halo(i): c.wait_send())
-        pl.when(has_next)(lambda c=halo(i): c.wait_recv())
-
-    near(range(rows - UP_ROWS, rows, 2))
-
     if nz > 3:
         relay(3, pass_second)
 
@@ -573,22 +567,29 @@
     lax.fori_loop(1, ny - 1, lambda o, c: (far(range(nt), o, z_rest, False), c)[1], 0)
     if nz > 1:
         far(range(nt), ny - 1, z_rest, False)
+    for i in range(len(HALO)):
+        pl.when(has_next)(lambda c=halo(i): c.wait_send())
+        pl.when(has_prev)(lambda c=halo(i): c.wait_recv())
+
+    near(range(0, UP_ROWS, 2))
+
     others(z_last)
     lax.fori_loop(1, ny - 1, lambda o, c: (far(range(nt), o, pl.ds(z_last, 1), False), c)[1], 0)
 
     def settle_row(zb, _):
-        across(0, zb, sent)
+        pl.when(zb == zi)(lambda: across(2, zb, sent))
+        pl.when(zb != zi)(lambda: across(0, zb, sent))
 
         @pl.when(zb <= zi)
         def _():
-            upward(0, zb * ny + yi, sent)
+            upward(2, zb * ny + yi, sent)
 
         @pl.when(zb >= zi)
         def _():
-            downward(0, zb * ny + yi, sent)
+            downward(2, zb * ny + yi, sent)
 
         def column(o, _):
-            block = zb * ny + o
+            block = zb * ny + (yi + o) % ny
 
             @pl.when(zb <= zi)
             def _():
@@ -600,13 +601,13 @@
 
             return 0
 
-        lax.fori_loop(0, ny, column, 0)
+        lax.fori_loop(1, ny, column, 0)
         return 0
 
     def head_copy(src, dst):
         return pltpu.make_async_remote_copy(
             src_ref=att.at[pl.ds(pl.multiple_of(dst * own_n, 16), own_n)], dst_ref=own.at[src],
-            send_sem=head_s.at[dst], recv_sem=head_r.at[src],
+            send_sem=head_s.at[(dst - src + nt - 1) % nt], recv_sem=head_r.at[(dst - src + nt - 1) % nt],
             device_id={"sp": sp, "tp": dst},
         )
 
@@ -618,7 +619,6 @@
     far(ours, ny - 1, pl.ds(z_last, 1), True)
     for p in ours[1:]:
         head_copy(tp, p).start()
-    across(1, zi, sent)
     lax.fori_loop(0, nz, settle_row, 0)
 
     def wait_gate(o, _):
@@ -637,7 +637,7 @@
     def settle(o, _):
         p = (tp + o) % nt
         head_copy(tp, p).wait_send()
-        head_copy(p, p).wait_recv()
+        head_copy(p, tp).wait_recv()
         return 0
 
     lax.fori_loop(1, nt, settle, 0)
@@ -696,7 +696,7 @@
             pltpu.VMEM((kt, d), BF16),
             pltpu.VMEM((kt, d), BF16),
             pltpu.VMEM((d, 3 * width), BF16),
-            pltpu.VMEM((d // 2 // 512, nt, 8, 512), BF16),
+            pltpu.VMEM((d // 2 // 512, nt, 8, 512), F32),
             pltpu.VMEM((nt, 8, d // 8), F32),
             pltpu.VMEM((8, d), F32),
             pltpu.VMEM((tokens, HEAD_DIM), F32),
@@ -704,7 +704,7 @@
             pltpu.VMEM((ny, ns // ny, c_here, 2 * width), BF16),
             pltpu.VMEM((tokens + halo, 2 * width), BF16),
             pltpu.VMEM((tokens, width), BF16),
-            pltpu.VMEM((UP_ROWS * GRID_W, d), BF16),
+            pltpu.VMEM((DOWN_ROWS * GRID_W, d), BF16),
             pltpu.VMEM((heads, TABLES + 3, GRID_W, PAIR), F32),
             pltpu.VMEM((heads, tokens, KEYS), F32),
             pltpu.VMEM((heads, tokens, ns // ny * c_here), F32),
@@ -716,12 +716,12 @@
             pltpu.VMEM((1, d), F32),
             pltpu.VMEM((1, d), F32),
             pltpu.VMEM(table.shape, F32),
-            sem((12 + 4 * (d // 2 // 512),)),
-            sem((d // 2 // 512, nt - 1)), sem((d // 2 // 512, nt - 1)), sem((nt - 1,)), sem((nt - 1,)),
-            sem((2 * (ns // ny), max(ny - 1, 1))), sem((2, ns + ns // ny)), sem((2, ns)),
+            sem((12 + d // 2 // 512,)),
+            sem((nt - 1,)), sem((nt - 1,)), sem((nt - 1,)), sem((nt - 1,)),
+            sem((ns // ny, max(ny - 1, 1))), sem((2, ns)), sem((2, ns)),
             sem((len(HALO),)), sem((len(HALO),)),
             sem((RAW_PARTS, 2 * (nt // CORES))), sem((RAW_PARTS, nt)),
-            sem((nt,)), sem((nt,)),
+            sem((nt - 1,)), sem((nt - 1,)),
         ],
         compiler_params=pltpu.CompilerParams(
             collective_id=0, has_side_effects=True, vmem_limit_bytes=VMEM_BYTES - tail

time: 35.6 us -> 33.3 us (0.935)
  Pallas kernels: 35.2 us -> 32.8 us
    pallas_call x1, Pallas kernels: 33.6 us -> 31.2 us  [shards(): pl.pallas_call(functools.partial(kernel, ns, nt, ny), out_shape=(pltpu.VM...]
where the time goes in v3:
time: 33.3 us; the launch traced here: 32.9 us
  Pallas kernels  32.8 us (98%)
    pallas_call x1, Pallas kernels, shards(): pl.pallas_call(functools.partial(kernel, ns, nt, ny), out_shape=(pltpu.VM...  31.2 us
    pallas_call x1, Pallas kernels, shards(): pl.pallas_call(finish, out_shape=jax.ShapeDtypeStruct((own_n, d), BF16),...  1.6 us

profile of v3, /device:TPU:1, one launch (start us, length us, event | category | flops | bytes accessed | tf_op | source)
XLA Modules:
  0.0 32.9 jit_solution(3289310449922389804)
XLA Ops:
  0.0 31.2 %shard_map.127 = (bf16[4,160,256]{2,1,0:T(8,128)(2,1)S(1)}, bf16[1024,2048]{1,0:T(8,128)(2,1)S(1)}, f32[1,2048]{1,0:T(1,128)S(1)}, bf16[160,2048]{1,0:T(8,128)(2,1)S(1)}) custom-call(f32[1,2048]{1,0:T(1,128)} %bitcast.5, f32[1,2048]{1,0:T(1,128)} %bitcast.6, f32[1,2048]{1,0:T(1,128)} %bitcast.7, f32[15,2,31]{2,1,0:T(2,128)} %bitcast.4, ...), custom_call_target="tpu_custom_call" | custom-call | tf_op jit(solution)/shard_map/pallas_call | solution.py:682
  31.2 1.6 %shard_map.128 = bf16[160,2048]{1,0:T(8,128)(2,1)} custom-call(bf16[4,160,256]{2,1,0:T(8,128)(2,1)S(1)} %get-tuple-element.9.own, bf16[1024,2048]{1,0:T(8,128)(2,1)S(1)} %get-tuple-element.10.wo, f32[1,2048]{1,0:T(1,128)S(1)} %get-tuple-element.11.gates, bf16[160,2048]{1,0:T(8,128)(2,1)S(1)} %get-tuple-element.12.lat_own), custom_call_target="tpu_custom_call" | custom-call | tf_op jit(solution)/shard_map/pallas_call | solution.py:733

commit v4 on v3

--- a/solution.py
+++ b/solution.py
@@ -23,7 +23,7 @@
 TABLES = 2 * WIN_ROWS - 2
 Z_FIRST = 3
 HALO = ((0, 2), (2, 2))
-ISSUE = ((), (0,), (), (1,))
+ISSUE = ((), ((0, 0),), (), (), ((1, 0),))
 RAW_PARTS = 1
 CORES = 2
 VMEM_BYTES = 67043328
@@ -45,7 +45,7 @@
     ns, nt, ny,
     cond_h, ctx_cond_h, gain_h, table_h,
     lat_h, ctx_h, wsh_h, wsc_h, wg_h, wq_h, wk_h, wv_h, wo_h,
-    own, wo, gates, lat_own,
+    own, wo, gates, lat_own, y_own,
     lat, ctx, wsh, wsc, wg, wqkv,
     modr, gater, mods, inv, hbuf, ctx_all, kv, q, raw, bias, s_near, s_far, acc, mx, att, lines,
     cond, ctx_cond, gain, table,
@@ -368,14 +368,19 @@
 
         lax.fori_loop(0, ny, one, 0)
 
+    def relay_down(k, pass_on):
+        @pl.when(zi + k < nz)
+        def _():
+            pass_on(zi + k, downward)
+
+    def relay_up(k, pass_on):
+        @pl.when(zi - k >= 0)
+        def _():
+            pass_on(zi - k, upward)
+
     def relay(k, pass_on):
-        @pl.when(zi + k < nz)
-        def _():
-            pass_on(zi + k, downward)
-
-        @pl.when(zi - k >= 0)
-        def _():
-            pass_on(zi - k, upward)
+        relay_down(k, pass_on)
+        relay_up(k, pass_on)
 
     across(1, zi, go)
     for part in range(2):
@@ -393,8 +398,9 @@
         )
 
     def send_halo(point):
-        for i in ISSUE[point]:
-            pl.when(has_next)(lambda c=halo(i): c.start())
+        for i, which in ISSUE[point]:
+            turn = (yi >= 0, yi == ny - 1, yi < ny - 1)[which]
+            pl.when(has_next & turn)(lambda c=halo(i): c.start())
 
     wq_load.wait()
     rest = (tokens - up_n) // 2
@@ -515,10 +521,6 @@
 
     everything = pl.ds(0, nz)
 
-    def far_all(o, _):
-        far(range(nt), o, everything, False)
-        return 0
-
     relay(1, pass_first)
     for i in range(1, RAW_PARTS):
         raw_along(i)
@@ -532,14 +534,25 @@
         raw_over(i)
     if nz > 2:
         relay(2, pass_second)
+    send_halo(4)
     for i in range(RAW_PARTS):
         raw_done(i)
     hbuf[0, 0:down_n, :] = modulate(raw[...], inv_of(raw[...]))
     below = dot(hbuf[0, 0:down_n, :], wqkv[:, 0:2 * width])
     kv[up_n + tokens:up_n + tokens + down_n, :] = below.astype(BF16)
-    near(range(rows - UP_ROWS, rows, 2))
+    up_pairs, down_pairs = range(0, UP_ROWS, 2), range(rows - UP_ROWS, rows, 2)
+
+    def halo_near():
+        for i in range(len(HALO)):
+            pl.when(has_prev)(lambda c=halo(i): c.wait_recv())
+        near(up_pairs)
+
     if nz > 3:
-        relay(3, pass_first)
+        relay_down(3, pass_first)
+    pl.when(my_half == 0)(lambda: near(down_pairs))
+    pl.when((my_half == 1) & (sp == 0))(lambda: near(up_pairs))
+    if nz > 3:
+        relay_up(3, pass_first)
     if nz > 3:
         relay(3, pass_second)
 
@@ -549,6 +562,8 @@
         return 0
 
     lax.fori_loop(4, nz, late_relay, 0)
+    theirs = [(1 - my_half) * half_t + j for j in range(half_t)]
+    ours = [my_half * half_t + (tp + o) % half_t for o in range(half_t)]
     low = zi < nz - nz // 2
     z_last = jnp.where(low, nz - 1, 0)
     z_rest = pl.ds(jnp.where(low, 0, 1), nz - 1)
@@ -560,21 +575,25 @@
 
         lax.fori_loop(1, ny, other, 0)
 
-    if ny > 1:
-        far_all(0, 0)
+    def middle(parts, zs):
+        lax.fori_loop(1, ny - 1, lambda o, c: (far(parts, o, zs, False), c)[1], 0)
+
+    def far_own(parts):
+        if ny > 1:
+            far(parts, 0, everything, False)
+
+    def far_rest(parts):
+        if nz > 1:
+            middle(parts, z_rest)
+            far(parts, ny - 1, z_rest, False)
+
+    far_own(theirs)
     for k in range(nz - 1):
         others(z_rest.start + k)
-    lax.fori_loop(1, ny - 1, lambda o, c: (far(range(nt), o, z_rest, False), c)[1], 0)
-    if nz > 1:
-        far(range(nt), ny - 1, z_rest, False)
-    for i in range(len(HALO)):
-        pl.when(has_next)(lambda c=halo(i): c.wait_send())
-        pl.when(has_prev)(lambda c=halo(i): c.wait_recv())
-
-    near(range(0, UP_ROWS, 2))
-
+    far_rest(theirs)
+    pl.when((my_half == 1) & (sp > 0))(halo_near)
     others(z_last)
-    lax.fori_loop(1, ny - 1, lambda o, c: (far(range(nt), o, pl.ds(z_last, 1), False), c)[1], 0)
+    middle(theirs, pl.ds(z_last, 1))
 
     def settle_row(zb, _):
         pl.when(zb == zi)(lambda: across(2, zb, sent))
@@ -611,14 +630,19 @@
             device_id={"sp": sp, "tp": dst},
         )
 
-    theirs = [(1 - my_half) * half_t + j for j in range(half_t)]
-    ours = [my_half * half_t + (tp + o) % half_t for o in range(half_t)]
     for p in theirs:
         far([p], ny - 1, pl.ds(z_last, 1), True)
         head_copy(tp, p).start()
+    pl.when(my_half == 0)(halo_near)
+    pl.when(my_half == 1)(lambda: near(down_pairs))
+    far_own(ours)
+    far_rest(ours)
+    middle(ours, pl.ds(z_last, 1))
     far(ours, ny - 1, pl.ds(z_last, 1), True)
     for p in ours[1:]:
         head_copy(tp, p).start()
+    for i in range(len(HALO)):
+        pl.when(has_next)(lambda c=halo(i): c.wait_send())
     lax.fori_loop(0, nz, settle_row, 0)
 
     def wait_gate(o, _):
@@ -630,28 +654,38 @@
     for i in range(1, nt):
         gsum = gsum + gater[i]
     gates[...] = jnp.concatenate([gsum[j:j + 1] for j in range(8)], axis=1)
-    own[tp] = att[my_rows, :]
     wo_load.wait()
     own_load.wait()
 
-    def settle(o, _):
-        p = (tp + o) % nt
+    def taken(p):
         head_copy(tp, p).wait_send()
         head_copy(p, tp).wait_recv()
-        return 0
-
-    lax.fori_loop(1, nt, settle, 0)
-
-
-def finish(own, wo, gates, lat_own, out, buf, sem):
-    nt = own.shape[0]
+
+    def part_of(p):
+        return pl.ds(pl.multiple_of(p * width, HEAD_DIM), width)
+
+    for n0 in range(0, d, step):
+        y_own[:, n0:n0 + step] = dot(att[my_rows, :], wo[part_of(tp), n0:n0 + step])
+    for p in ours[1:]:
+        taken(p)
+        for n0 in range(0, d, step):
+            y_own[:, n0:n0 + step] += dot(own[p], wo[part_of(p), n0:n0 + step])
+    for p in theirs:
+        taken(p)
+
+
+def finish(own, wo, gates, lat_own, y_own, out, buf, sem):
+    nt, _, width = own.shape
     d = wo.shape[1]
     step = d // 4
-    a = jnp.concatenate([own[i] for i in range(nt)], axis=1)
+    half_t = nt // 2
+    other = (1 - lax.axis_index("tp") // half_t) * half_t
+    a = jnp.concatenate([own[other + i] for i in range(half_t)], axis=1)
+    rows = pl.ds(pl.multiple_of(other * width, HEAD_DIM), half_t * width)
     copies = []
     for i in range(4):
         cols = pl.ds(i * step, step)
-        y = dot(a, wo[:, cols])
+        y = y_own[:, cols] + dot(a, wo[rows, cols])
         buf[:, cols] = (lat_own[:, cols].astype(F32) + gates[:, cols] * y).astype(BF16)
         copies.append(pltpu.make_async_copy(buf.at[:, cols], out.at[:, cols], sem.at[i]))
         copies[-1].start()
@@ -686,9 +720,10 @@
             pltpu.VMEM(out_weight.shape, BF16),
             pltpu.VMEM((1, d), F32),
             pltpu.VMEM((own_n, d), BF16),
+            pltpu.VMEM((own_n, d), F32),
         ),
         in_specs=[hbm] * 13,
-        out_specs=(vmem,) * 4,
+        out_specs=(vmem,) * 5,
         scratch_shapes=[
             pltpu.VMEM((tokens, d), BF16),
             pltpu.VMEM((c_here, d), BF16),
@@ -733,7 +768,7 @@
     return pl.pallas_call(
         finish,
         out_shape=jax.ShapeDtypeStruct((own_n, d), BF16),
-        in_specs=[vmem] * 4,
+        in_specs=[vmem] * 5,
         out_specs=hbm,
         scratch_shapes=[pltpu.VMEM((own_n, d), BF16), sem((4,))],
         compiler_params=pltpu.CompilerParams(vmem_limit_bytes=16 * 1024 * 1024),

time: 33.3 us -> 32.5 us (0.976)
  Pallas kernels: 32.8 us -> 32.2 us
where the time goes in v4:
time: 32.5 us; the launch traced here: 32.4 us
  Pallas kernels  32.2 us (99%)
    pallas_call x1, Pallas kernels, shards(): pl.pallas_call(functools.partial(kernel, ns, nt, ny), out_shape=(pltpu.VM...  30.9 us
    pallas_call x1, Pallas kernels, shards(): pl.pallas_call(finish, out_shape=jax.ShapeDtypeStruct((own_n, d), BF16),...  1.31 us

profile of v4, /device:TPU:1, one launch (start us, length us, event | category | flops | bytes accessed | tf_op | source)
XLA Modules:
  0.0 32.4 jit_solution(2877352516247709259)
XLA Ops:
  0.0 30.9 %shard_map.127 = (bf16[4,160,256]{2,1,0:T(8,128)(2,1)S(1)}, bf16[1024,2048]{1,0:T(8,128)(2,1)S(1)}, f32[1,2048]{1,0:T(1,128)S(1)}, bf16[160,2048]{1,0:T(8,128)(2,1)S(1)}, f32[160,2048]{1,0:T(8,128)S(1)}) custom-call(f32[1,2048]{1,0:T(1,128)} %bitcast.5, f32[1,2048]{1,0:T(1,128)} %bitcast.6, f32[1,2048]{1,0:T(1,128)} %bitcast.7, f32[15,2,31]{2,1,0:T(2,128)} %bitcast.4, ...), custom_call_target="tpu_custom_call" | custom-call | tf_op jit(solution)/shard_map/pallas_call | solution.py:716
  30.9 1.3 %shard_map.128 = bf16[160,2048]{1,0:T(8,128)(2,1)} custom-call(bf16[4,160,256]{2,1,0:T(8,128)(2,1)S(1)} %get-tuple-element.10.own, bf16[1024,2048]{1,0:T(8,128)(2,1)S(1)} %get-tuple-element.11.wo, f32[1,2048]{1,0:T(1,128)S(1)} %get-tuple-element.12.gates, bf16[160,2048]{1,0:T(8,128)(2,1)S(1)} %get-tuple-element.13.lat_own, ...), custom_call_target="tpu_custom_call" | custom-call | tf_op jit(solution)/shard_map/pallas_call | solution.py:768

commit v5 on v4

--- a/solution.py
+++ b/solution.py
@@ -527,6 +527,8 @@
     near(range(UP_ROWS, rows - UP_ROWS, 2))
     relay(1, pass_second)
     send_halo(2)
+    up_pairs, down_pairs = range(0, UP_ROWS, 2), range(rows - UP_ROWS, rows, 2)
+    pl.when(sp == 0)(lambda: near(up_pairs))
     if nz > 2:
         relay(2, pass_first)
     send_halo(3)
@@ -540,17 +542,15 @@
     hbuf[0, 0:down_n, :] = modulate(raw[...], inv_of(raw[...]))
     below = dot(hbuf[0, 0:down_n, :], wqkv[:, 0:2 * width])
     kv[up_n + tokens:up_n + tokens + down_n, :] = below.astype(BF16)
-    up_pairs, down_pairs = range(0, UP_ROWS, 2), range(rows - UP_ROWS, rows, 2)
 
     def halo_near():
         for i in range(len(HALO)):
-            pl.when(has_prev)(lambda c=halo(i): c.wait_recv())
+            halo(i).wait_recv()
         near(up_pairs)
 
     if nz > 3:
         relay_down(3, pass_first)
     pl.when(my_half == 0)(lambda: near(down_pairs))
-    pl.when((my_half == 1) & (sp == 0))(lambda: near(up_pairs))
     if nz > 3:
         relay_up(3, pass_first)
     if nz > 3:
@@ -591,7 +591,7 @@
     for k in range(nz - 1):
         others(z_rest.start + k)
     far_rest(theirs)
-    pl.when((my_half == 1) & (sp > 0))(halo_near)
+    pl.when((my_half == 1) & has_prev)(halo_near)
     others(z_last)
     middle(theirs, pl.ds(z_last, 1))
 
@@ -633,14 +633,15 @@
     for p in theirs:
         far([p], ny - 1, pl.ds(z_last, 1), True)
         head_copy(tp, p).start()
-    pl.when(my_half == 0)(halo_near)
+    pl.when((my_half == 0) & has_prev)(halo_near)
     pl.when(my_half == 1)(lambda: near(down_pairs))
     far_own(ours)
     far_rest(ours)
     middle(ours, pl.ds(z_last, 1))
-    far(ours, ny - 1, pl.ds(z_last, 1), True)
+    far(ours[1:], ny - 1, pl.ds(z_last, 1), True)
     for p in ours[1:]:
         head_copy(tp, p).start()
+    far(ours[:1], ny - 1, pl.ds(z_last, 1), True)
     for i in range(len(HALO)):
         pl.when(has_next)(lambda c=halo(i): c.wait_send())
     lax.fori_loop(0, nz, settle_row, 0)
@@ -657,21 +658,19 @@
     wo_load.wait()
     own_load.wait()
 
-    def taken(p):
-        head_copy(tp, p).wait_send()
-        head_copy(p, tp).wait_recv()
-
     def part_of(p):
         return pl.ds(pl.multiple_of(p * width, HEAD_DIM), width)
 
     for n0 in range(0, d, step):
         y_own[:, n0:n0 + step] = dot(att[my_rows, :], wo[part_of(tp), n0:n0 + step])
     for p in ours[1:]:
-        taken(p)
+        head_copy(p, tp).wait_recv()
         for n0 in range(0, d, step):
             y_own[:, n0:n0 + step] += dot(own[p], wo[part_of(p), n0:n0 + step])
     for p in theirs:
-        taken(p)
+        head_copy(p, tp).wait_recv()
+    for p in theirs + ours[1:]:
+        head_copy(tp, p).wait_send()
 
 
 def finish(own, wo, gates, lat_own, y_own, out, buf, sem):

time: 32.5 us -> 32.6 us (level)
  no operation moved by 1% of the time
where the time goes in v5:
time: 32.6 us; the launch traced here: 32.4 us
  Pallas kernels  32.2 us (99%)
    pallas_call x1, Pallas kernels, shards(): pl.pallas_call(functools.partial(kernel, ns, nt, ny), out_shape=(pltpu.VM...  30.9 us
    pallas_call x1, Pallas kernels, shards(): pl.pallas_call(finish, out_shape=jax.ShapeDtypeStruct((own_n, d), BF16),...  1.3 us

profile of v5, /device:TPU:1, one launch (start us, length us, event | category | flops | bytes accessed | tf_op | source)
XLA Modules:
  0.0 32.4 jit_solution(777019602644013111)
XLA Ops:
  0.0 30.9 %shard_map.127 = (bf16[4,160,256]{2,1,0:T(8,128)(2,1)S(1)}, bf16[1024,2048]{1,0:T(8,128)(2,1)S(1)}, f32[1,2048]{1,0:T(1,128)S(1)}, bf16[160,2048]{1,0:T(8,128)(2,1)S(1)}, f32[160,2048]{1,0:T(8,128)S(1)}) custom-call(f32[1,2048]{1,0:T(1,128)} %bitcast.5, f32[1,2048]{1,0:T(1,128)} %bitcast.6, f32[1,2048]{1,0:T(1,128)} %bitcast.7, f32[15,2,31]{2,1,0:T(2,128)} %bitcast.4, ...), custom_call_target="tpu_custom_call" | custom-call | tf_op jit(solution)/shard_map/pallas_call | solution.py:715
  30.9 1.3 %shard_map.128 = bf16[160,2048]{1,0:T(8,128)(2,1)} custom-call(bf16[4,160,256]{2,1,0:T(8,128)(2,1)S(1)} %get-tuple-element.10.own, bf16[1024,2048]{1,0:T(8,128)(2,1)S(1)} %get-tuple-element.11.wo, f32[1,2048]{1,0:T(1,128)S(1)} %get-tuple-element.12.gates, bf16[160,2048]{1,0:T(8,128)(2,1)S(1)} %get-tuple-element.13.lat_own, ...), custom_call_target="tpu_custom_call" | custom-call | tf_op jit(solution)/shard_map/pallas_call | solution.py:767

commit v6 on v5

--- a/solution.py
+++ b/solution.py
@@ -23,7 +23,7 @@
 TABLES = 2 * WIN_ROWS - 2
 Z_FIRST = 3
 HALO = ((0, 2), (2, 2))
-ISSUE = ((), ((0, 0),), (), (), ((1, 0),))
+ISSUE = ((), ((0, 0), (1, 2)), (), (), ((1, 1),))
 RAW_PARTS = 1
 CORES = 2
 VMEM_BYTES = 67043328

time: 32.6 us -> 32.6 us (level)
  no operation moved by 1% of the time
where the time goes in v6:
time: 32.6 us; the launch traced here: 32.4 us
  Pallas kernels  32.2 us (99%)
    pallas_call x1, Pallas kernels, shards(): pl.pallas_call(functools.partial(kernel, ns, nt, ny), out_shape=(pltpu.VM...  30.9 us
    pallas_call x1, Pallas kernels, shards(): pl.pallas_call(finish, out_shape=jax.ShapeDtypeStruct((own_n, d), BF16),...  1.3 us

profile of v6, /device:TPU:1, one launch (start us, length us, event | category | flops | bytes accessed | tf_op | source)
XLA Modules:
  0.0 32.4 jit_solution(11041722830594846024)
XLA Ops:
  0.0 30.9 %shard_map.127 = (bf16[4,160,256]{2,1,0:T(8,128)(2,1)S(1)}, bf16[1024,2048]{1,0:T(8,128)(2,1)S(1)}, f32[1,2048]{1,0:T(1,128)S(1)}, bf16[160,2048]{1,0:T(8,128)(2,1)S(1)}, f32[160,2048]{1,0:T(8,128)S(1)}) custom-call(f32[1,2048]{1,0:T(1,128)} %bitcast.5, f32[1,2048]{1,0:T(1,128)} %bitcast.6, f32[1,2048]{1,0:T(1,128)} %bitcast.7, f32[15,2,31]{2,1,0:T(2,128)} %bitcast.4, ...), custom_call_target="tpu_custom_call" | custom-call | tf_op jit(solution)/shard_map/pallas_call | solution.py:715
  30.9 1.3 %shard_map.128 = bf16[160,2048]{1,0:T(8,128)(2,1)} custom-call(bf16[4,160,256]{2,1,0:T(8,128)(2,1)S(1)} %get-tuple-element.10.own, bf16[1024,2048]{1,0:T(8,128)(2,1)S(1)} %get-tuple-element.11.wo, f32[1,2048]{1,0:T(1,128)S(1)} %get-tuple-element.12.gates, bf16[160,2048]{1,0:T(8,128)(2,1)S(1)} %get-tuple-element.13.lat_own, ...), custom_call_target="tpu_custom_call" | custom-call | tf_op jit(solution)/shard_map/pallas_call | solution.py:767
